TPU v7x, 256 devices: a whole 4x4x8 slice. The times are simulated.
256 devices in a mesh: fs: 32 (over z, y), tp: 8 (over x, core).
Axes of the slice: x: 4, y: 4, z: 8, core: 2. Of those that a mesh axis runs over, the one named last changes fastest.
Arguments:
- tokens: bfloat16 [32768, 2048], P('fs', 'tp'), may hold values from -6 to 6
- mixer_gain: float32 [2048], replicated, may hold values from 0.1 to 1.9
- conv_taps: bfloat16 [3, 1024], replicated, may hold values from -3.5 to 3.5
- outer_weight: bfloat16 [2048, 1024], P('fs', 'tp'), may hold values from -0.125 to 0.125
- inner_weight: bfloat16 [2048, 1024], P('fs', 'tp'), may hold values from -0.125 to 0.125
- value_weight: bfloat16 [2048, 1024], P('fs', 'tp'), may hold values from -0.125 to 0.125
- merge_weight: bfloat16 [1024, 2048], P('tp', 'fs'), may hold values from -0.375 to 0.375
- merge_gain: float32 [2048], replicated, may hold values from 0.1 to 1.9
- channel_gain: float32 [2048], replicated, may hold values from 0.1 to 1.9
- gate_weight: bfloat16 [2048, 5632], P('fs', 'tp'), may hold values from -0.125 to 0.125
- up_weight: bfloat16 [2048, 5632], P('fs', 'tp'), may hold values from -0.125 to 0.125
- down_weight: bfloat16 [5632, 2048], P('tp', 'fs'), may hold values from -0.15625 to 0.15625
- output_gain: float32 [2048], replicated, may hold values from 0.1 to 1.9
Outputs:
- layer_out: bfloat16 [32768, 2048], P('fs', 'tp')
All inputs are finite; a program needn't handle non-finite values.
Results may differ from a plain program's by a relative error of at most 0.018.
Values may be sent and summed in bfloat16 or wider, within the bound.
No kernel may reach another device: no remote copies, remote signals or barrier semaphores. Data moves between devices by JAX's collectives and lax.ppermute only.
A program may use at most 128 MiB of HBM per device.

v0:
```python
import jax
import jax.numpy as jnp
from jax import lax
from jax.experimental import pallas as pl
from jax.experimental.pallas import tpu as pltpu
from jax.sharding import Mesh
from jax.sharding import PartitionSpec as P

TP = ("tp_0", "tp_1")
FS = ("fs_0", "fs_1")
EPS = 1e-06
HALO = 32
F32 = jnp.float32
BF16 = jnp.bfloat16


def shift(value, axis, by):
    n = lax.axis_size(axis)
    return lax.ppermute(value, axis, [(i, (i + by) % n) for i in range(n)])


def around(value, axis, *held, cut=None):
    half = cut or value.shape[0] // 2
    left = shift(value, axis, 1)
    right = shift(value, axis, -1)
    left, right, *held = lax.optimization_barrier((left, right, *held))
    far_low = shift(left[:half], axis, 1)
    far_high = shift(right[half:], axis, -1)
    return value, left, right, far_low, far_high, *held


def copy_for_each(value, axis):
    n = lax.axis_size(axis)
    return lax.all_to_all(
        jnp.broadcast_to(value[None], (n, *value.shape)), axis, 0, 0, tiled=True
    )


def scatter_sum(own, to_right, to_left, keep_right, keep_left):
    half = own.shape[0] // 2
    from_left = shift(to_right, "tp_0", 1)
    from_right = shift(to_left, "tp_0", -1)
    add = lambda a, b: (a.astype(F32) + b.astype(F32)).astype(BF16)
    low = shift(add(keep_right, from_left[:half]), "tp_0", 1)
    high = shift(add(keep_left, from_right[:half]), "tp_0", -1)
    low, high, from_left, from_right = lax.optimization_barrier((low, high, from_left, from_right))
    top = own[:half].astype(F32) + from_right[half:].astype(F32) + low.astype(F32)
    bottom = own[half:].astype(F32) + from_left[half:].astype(F32) + high.astype(F32)
    return jnp.concatenate([top, bottom], axis=0).astype(BF16)


def put_pieces(j, half, block, own, to_right, to_left, keep_right, keep_left, rows):
    if j == 0:
        own[rows, :] = block
    elif j == 1:
        if half == 0:
            keep_right[...] = block
        else:
            to_right[rows, :] = block
    elif j == 2:
        if half == 0:
            to_right[: block.shape[0], :] = block
        else:
            to_left[: block.shape[0], :] = block
    else:
        if half == 0:
            to_left[block.shape[0] :, :] = block
        else:
            keep_left[...] = block


def dot_nt(a, b):
    return lax.dot_general(a, b, (((1,), (1,)), ((), ())), preferred_element_type=F32)


PARTS_Y = ((0, 0, 8), (3, 0, 8), (1, 0, 8), (2, 0, 4), (2, 4, 8))


def mixer_kernel(
    place, own, left, right, low, high, *rest
):
    pieces, rest = rest[:10], rest[10:]
    taps, gain, o_own, o_right, o_left, o_keep_right, o_keep_left = rest[:7]
    weights, normed, outer, signal, mixed, sems = rest[7:]
    x, k, y = place[0], place[1], place[2]
    copies = []
    for side in range(2):
        slot = k if side == 0 else 1 - k
        for q, (turn, begin, end) in enumerate(PARTS_Y):
            at = lax.rem(y + turn, 4)
            for b in range(begin, end):
                row = pl.multiple_of((b * 4 + at) * 64, 64)
                copies.append(
                    pltpu.make_async_copy(
                        pieces[side * 5 + q].at[b - begin],
                        weights.at[slot, pl.ds(row, 64), :],
                        sems.at[len(copies)],
                    )
                )
    for copy in copies:
        copy.start()
    half = normed.shape[0] // 2
    positions = [lax.rem(x + j, 4) for j in range(4)]
    for i, (begin, size, steps) in enumerate(((0, 96, 3), (288, 64, 4))):

        @pl.loop(0, steps)
        def _(tile):
            at = pl.multiple_of(tile * size, 32)
            r, h = pl.ds(begin + at, size), pl.ds(at, size)
            floats = [b.astype(F32) for b in (own[r, :], right[r, :], (low if i == 0 else high)[h, :], left[r, :])]
            squares = sum(jnp.sum(f * f, axis=1, keepdims=True) for f in floats)
            factor = lax.rsqrt(squares * (1.0 / 2048) + EPS)
            for j in range(4):
                g = gain[pl.ds(positions[j], 1), :]
                start = pl.multiple_of(positions[j] * 512, 512)
                normed[r, pl.ds(start, 512)] = (floats[j] * factor * g).astype(BF16)

    for copy in copies:
        copy.wait()
    signal[0:8, :] = jnp.zeros((8, 256), F32)

    @pl.loop(0, 2)
    def _(i):
        at = pl.multiple_of(i * half, 16)
        for c in range(2):
            ch = slice(c * 128, (c + 1) * 128)
            product = jnp.dot(normed[pl.ds(at, half), :], weights[c, :, 0:384], preferred_element_type=F32)
            outer[pl.ds(at, half), ch] = product[:, 0:128]
            signal[pl.ds(at + 8, half), ch] = product[:, 128:256] * product[:, 256:384]

    base = pl.multiple_of(k * HALO, HALO)

    @pl.loop(0, 2)
    def _(tile):
        at = pl.multiple_of(tile * 256, 256)
        for c in range(2):
            ch = slice(c * 128, (c + 1) * 128)
            s = signal[pl.ds(base + at, 264), ch]
            t = taps[:, ch]
            conv = t[0:1] * s[6:262] + t[1:2] * s[7:263] + t[2:3] * s[8:264]
            gated = outer[pl.ds(base + at, 256), ch] * conv
            scale = lax.rsqrt(jnp.mean(gated * gated, axis=1, keepdims=True) + EPS)
            mixed[pl.ds(at, 256), ch] = (gated * scale).astype(BF16)

    for j in range(4):
        start = pl.multiple_of(positions[j] * 512, 512)
        for zz in range(2):
            n = pl.ds(start + zz * 256, 256)
            w = jnp.concatenate([weights[0, n, 384:512], weights[1, n, 384:512]], axis=1)
            share = dot_nt(mixed[...], w).astype(BF16)
            cols = slice(zz * 256, (zz + 1) * 256)
            for h in range(2):
                put_pieces(
                    j, h, share[h * 256 : (h + 1) * 256],
                    *(ref.at[:, cols] for ref in (o_own, o_right, o_left, o_keep_right, o_keep_left)),
                    slice(h * 256, (h + 1) * 256),
                )


def norm_kernel(
    place, t_own, t_left, t_right, t_far, m_own, m_left, m_right, m_low, m_high,
    merge_gain, channel_gain, arrived, normed, o_first, near, sem,
):
    copy = pltpu.make_async_copy(arrived, near, sem)
    copy.start()
    x, k = place[0], place[1]
    positions = [lax.rem(x + j, 4) for j in range(4)]
    base = pl.multiple_of(k * HALO, HALO)
    for i in range(2):

        @pl.loop(0, 8)
        def _(tile):
            at = pl.multiple_of(tile * 32, 32)
            r, h = pl.ds(i * 256 + at, 32), pl.ds(at, 32)
            tr = pl.ds(base + i * 256 + at, 32)
            merged = [b.astype(F32) for b in (m_own[r, :], m_right[r, :], (m_low if i == 0 else m_high)[h, :], m_left[r, :])]
            toks = [b[tr, :].astype(F32) for b in (t_own, t_right, t_far, t_left)]
            squares = sum(jnp.sum(f * f, axis=1, keepdims=True) for f in merged)
            factor = lax.rsqrt(squares * (1.0 / 2048) + EPS)
            first = []
            for j in range(4):
                g = merge_gain[pl.ds(positions[j], 1), :]
                first.append((toks[j] + merged[j] * factor * g).astype(BF16))
            o_first[r, :] = first[0]
            first = [f.astype(F32) for f in first]
            squares = sum(jnp.sum(f * f, axis=1, keepdims=True) for f in first)
            factor = lax.rsqrt(squares * (1.0 / 2048) + EPS)
            for j in range(4):
                g = channel_gain[pl.ds(positions[j], 1), :]
                start = pl.multiple_of(positions[j] * 512, 512)
                normed[r, pl.ds(start, 512)] = (first[j] * factor * g).astype(BF16)

    copy.wait()


def pack_kernel(gate, up, down, out):
    out[:, 0:640] = gate[:, 0:640]
    out[:, 640:1280] = up[:, 0:640]
    out[:, 1280:1408] = jnp.concatenate([gate[:, 640:704], up[:, 640:704]], axis=1)
    out[:, 1408:2048] = down[:, 0:640]
    out[:, 2048:2176] = jnp.concatenate([down[:, 640:704], jnp.zeros((64, 64), BF16)], axis=1)


def forward_kernel(place, normed, weights, out):
    x = place[0]
    lane = lax.broadcasted_iota(jnp.int32, (256, 128), 1)

    @pl.loop(0, 2)
    def _(i):
        r = pl.ds(pl.multiple_of(i * 256, 256), 256)
        both = jnp.dot(normed[r, :], weights[:, 0:1408], preferred_element_type=F32)
        gate, up, tail = both[:, 0:640], both[:, 640:1280], both[:, 1280:1408]
        hidden = (gate / (1.0 + jnp.exp(-gate)) * up).astype(BF16)
        other = pltpu.roll(tail, 64, 1)
        last = jnp.where(lane < 64, tail / (1.0 + jnp.exp(-tail)) * other, 0.0)
        hidden = jnp.concatenate([hidden, last.astype(BF16)], axis=1)
        for j in range(4):
            start = pl.multiple_of(lax.rem(x + j, 4) * 512, 512)
            for zz in range(2):
                n = pl.ds(start + zz * 256, 256)
                out[j, r, zz * 256 : (zz + 1) * 256] = dot_nt(hidden, weights[n, 1408:2176]).astype(BF16)


VM = pl.BlockSpec(memory_space=pltpu.VMEM)
SM = pl.BlockSpec(memory_space=pltpu.SMEM)
HB = pl.BlockSpec(memory_space=pltpu.HBM)
SHARES = [
    jax.ShapeDtypeStruct((512, 512), BF16),
    jax.ShapeDtypeStruct((512, 512), BF16),
    jax.ShapeDtypeStruct((512, 512), BF16),
    jax.ShapeDtypeStruct((256, 512), BF16),
    jax.ShapeDtypeStruct((256, 512), BF16),
]


def shards(
    tokens, mixer_gain, conv_taps, outer_weight, inner_weight, value_weight, merge_weight,
    merge_gain, channel_gain, gate_weight, up_weight, down_weight, output_gain,
):
    x, k = lax.axis_index("tp_0"), lax.axis_index("tp_1")
    y = lax.axis_index("fs_1")
    place = jnp.stack([x, k, y]).astype(jnp.int32)
    span = 512 + HALO

    first_weights = jnp.concatenate([outer_weight, inner_weight, value_weight, merge_weight.T], axis=1)
    second_weights = pl.pallas_call(
        pack_kernel, out_shape=jax.ShapeDtypeStruct((64, 2176), BF16), in_specs=[VM] * 3, out_specs=VM
    )(gate_weight, up_weight, down_weight.T)
    second = lax.all_gather(second_weights, FS, axis=0, tiled=True)

    kept = lax.dynamic_slice_in_dim(tokens, k * (512 - HALO), span, 0)
    given = lax.dynamic_slice_in_dim(tokens, (1 - k) * (512 - HALO), span, 0)
    taken = shift(given, "tp_1", 1)
    block = jnp.where(k == 0, jnp.concatenate([kept, taken], 1), jnp.concatenate([taken, kept], 1))
    t_own, t_left, t_right, t_low, t_high = around(block, "tp_0", cut=288)

    plane = copy_for_each(first_weights, "fs_0")
    near = around(plane, "fs_1")
    near_other = [shift(part, "tp_1", 1) for part in near]

    own_taps = lax.dynamic_slice_in_dim(conv_taps, x * 256, 256, 1).astype(F32)
    pieces = pl.pallas_call(
        mixer_kernel,
        out_shape=SHARES,
        in_specs=[SM] + [VM] * 5 + [HB] * 10 + [VM] * 2,
        out_specs=[VM] * 5,
        scratch_shapes=[
            pltpu.VMEM((2, 2048, 512), BF16),
            pltpu.VMEM((span, 2048), BF16),
            pltpu.VMEM((span, 256), F32),
            pltpu.VMEM((span + 8, 256), F32),
            pltpu.VMEM((512, 256), BF16),
            pltpu.SemaphoreType.DMA((64,)),
        ],
        compiler_params=pltpu.CompilerParams(vmem_limit_bytes=26 * 2**20),
        cost_estimate=pl.CostEstimate(flops=2_300_000_000, bytes_accessed=9_000_000, transcendentals=0),
    )(place, t_own, t_left, t_right, t_low, t_high, *near, *near_other, own_taps, mixer_gain.reshape(4, 512))
    merged = scatter_sum(*pieces)
    *gathered, second = around(merged, "tp_0", second)

    normed, first, second = pl.pallas_call(
        norm_kernel,
        out_shape=[
            jax.ShapeDtypeStruct((512, 2048), BF16),
            jax.ShapeDtypeStruct((512, 512), BF16),
            jax.ShapeDtypeStruct((2048, 2176), BF16),
        ],
        in_specs=[SM] + [VM] * 11 + [HB],
        out_specs=[VM] * 3,
        scratch_shapes=[pltpu.SemaphoreType.DMA],
        compiler_params=pltpu.CompilerParams(vmem_limit_bytes=32 * 2**20),
        cost_estimate=pl.CostEstimate(flops=30_000_000, bytes_accessed=6_500_000, transcendentals=0),
    )(
        place, t_own, t_left, t_right, jnp.concatenate([t_low, t_high], 0), *gathered,
        merge_gain.reshape(4, 512), channel_gain.reshape(4, 512), second,
    )
    forward = pl.pallas_call(
        forward_kernel,
        out_shape=jax.ShapeDtypeStruct((4, 512, 512), BF16),
        in_specs=[SM] + [VM] * 2,
        out_specs=VM,
        compiler_params=pltpu.CompilerParams(vmem_limit_bytes=20 * 2**20),
        cost_estimate=pl.CostEstimate(flops=4_500_000_000, bytes_accessed=13_000_000, transcendentals=0),
    )
    theirs = shift(forward(place, shift(normed, "tp_1", 1), second), "tp_1", 1).astype(F32)
    ours = forward(place, normed, second).astype(F32) + theirs
    ours = ours.astype(BF16)
    pieces = (
        ours[0],
        jnp.concatenate([ours[2, :256], ours[1, 256:]], 0),
        jnp.concatenate([ours[2, 256:], ours[3, :256]], 0),
        ours[1, :256],
        ours[3, 256:],
    )
    down = scatter_sum(*pieces).astype(F32)
    squares = jnp.sum(down * down, axis=1).reshape(1, 4, 128)
    total = lax.all_to_all(jnp.broadcast_to(squares, (4, 4, 128)), "tp_0", 0, 0, tiled=True).sum(0)
    factor = lax.rsqrt(total.reshape(512, 1) / 2048 + EPS)
    own_gain = lax.dynamic_slice_in_dim(output_gain, x * 512, 512)
    result = (first.astype(F32) + down * factor * own_gain).astype(BF16)
    kept = lax.dynamic_slice_in_dim(result, k * 256, 256, 1)
    given = lax.dynamic_slice_in_dim(result, (1 - k) * 256, 256, 1)
    taken = shift(given, "tp_1", 1)
    return jnp.where(k == 0, jnp.concatenate([kept, taken], 0), jnp.concatenate([taken, kept], 0))


def solution(mesh):
    finer = Mesh(mesh.devices.reshape(8, 4, 4, 2), ("fs_0", "fs_1", "tp_0", "tp_1"))
    wide, tall = P(FS, TP), P(TP, FS)
    placed = (wide, P(), P(), wide, wide, wide, tall, P(), P(), wide, wide, tall, P())
    named = lambda *args: shards(*args)
    return jax.shard_map(named, mesh=finer, in_specs=placed, out_specs=P(FS, TP), check_vma=False)
```

profile of v0, /device:TPU:1, one launch (start us, length us, event | category | flops | bytes accessed | tf_op | source)
XLA Modules:
  0.0 195.2 jit_solution(15616881589481398429)
XLA Ops:
  6.5 1.8 shard_map.128
  8.4 0.8 pad_maximum_fusion.5
  9.2 0.8 broadcast_in_dim.6
  10.0 9.0 %all-to-all-start = ((bf16[8,64,512]{2,1,0:T(8,128)(2,1)}), bf16[8,64,512]{2,1,0:T(8,128)(2,1)S(1)}, u32[]{:S(2)}, u32[]{:S(2)}) async-start(bf16[8,64,512]{2,1,0:T(8,128)(2,1)} %broadcast_in_dim.6), calls=%async_computation | async-start | bytes 1048576 | tf_op jit(solution)/shard_map/all_to_all | solution.py:34
  19.1 1.0 collective-permute-start
  20.1 1.2 collective-permute-done
  21.4 1.3 collective-permute-start.1
  22.7 1.5 collective-permute-start.2
  24.2 14.3 %all-to-all-done.rest_0_ = bf16[8,64,512]{2,1,0:T(8,128)(2,1)S(1)} async-done(((bf16[8,64,512]{2,1,0:T(8,128)(2,1)}), bf16[8,64,512]{2,1,0:T(8,128)(2,1)S(1)}, u32[]{:S(2)}, u32[]{:S(2)}) %all-to-all-start) | async-done | bytes 524320 | tf_op jit(solution)/shard_map/all_to_all | solution.py:34
  38.5 1.5 collective-permute-start.5
  40.0 1.6 collective-permute-start.6
  41.6 1.3 collective-permute-start.3
  43.0 1.5 collective-permute-start.4
  44.5 1.5 collective-permute-start.9
  46.0 8.8 %collective-permute-done.5.rest_1_ = bf16[8,64,512]{2,1,0:T(8,128)(2,1)S(1)} collective-permute-done((bf16[8,64,512]{2,1,0:T(8,128)(2,1)S(1)}, bf16[8,64,512]{2,1,0:T(8,128)(2,1)S(1)}, u32[]{:S(2)}, u32[]{:S(2)}) %collective-permute-start.5) | collective-permute-done | bytes 524320 | tf_op jit(solution)/shard_map/ppermute | solution.py:19
  55.1 1.0 slice.80
  56.1 2.5 %collective-permute-start.8 = (bf16[4,64,512]{2,1,0:T(8,128)(2,1)S(1)}, bf16[4,64,512]{2,1,0:T(8,128)(2,1)}, u32[]{:S(2)}, u32[]{:S(2)}) collective-permute-start(bf16[4,64,512]{2,1,0:T(8,128)(2,1)S(1)} %slice.80), channel_id=1, source_target_pairs={{0,24},{8,0},{16,8},{24,16},{1,25},{9,1},{17,9},{25,17},{2,26},{10... | collective-permute-start | bytes 786440 | tf_op jit(solution)/shard_map/ppermute | solution.py:19
  58.6 1.4 collective-permute-start.10
  60.1 3.1 %collective-permute-done.7.rest_3_ = bf16[4,64,512]{2,1,0:T(8,128)(2,1)S(1)} collective-permute-done((bf16[4,64,512]{2,1,0:T(8,128)(2,1)S(1)}, bf16[4,64,512]{2,1,0:T(8,128)(2,1)S(1)}, u32[]{:S(2)}, u32[]{:S(2)}) %collective-permute-start.7) | collective-permute-done | bytes 262176 | tf_op jit(solution)/shard_map/ppermute | solution.py:19
  63.2 1.7 collective-permute-start.12
  66.7 8.4 %shard_map.127 = (bf16[512,512]{1,0:T(8,128)(2,1)S(1)}, bf16[512,512]{1,0:T(8,128)(2,1)S(1)}, bf16[512,512]{1,0:T(8,128)(2,1)S(1)}, bf16[256,512]{1,0:T(8,128)(2,1)S(1)}, bf16[256,512]{1,0:T(8,128)(2,1)S(1)}) custom-call(s32[3]{0:T(128)S(1)} %pad_add_fusion.place, bf16[544,512]{1,0:T(8,128)(2,1)S(1)} %maximum_select_fusion.own.t_own, ...), custom_call_target="tpu_custom_call" | custom-call | flops 2300000000 | bytes 9000000 | tf_op jit(solution)/shard_map/pallas_call | solution.py:262
  75.1 2.7 %collective-permute-start.16 = (bf16[512,512]{1,0:T(8,128)(2,1)S(1)}, bf16[512,512]{1,0:T(8,128)(2,1)S(1)}, u32[]{:S(2)}, u32[]{:S(2)}) collective-permute-start(bf16[512,512]{1,0:T(8,128)(2,1)S(1)} %get-tuple-element.36), channel_id=1, source_target_pairs={{0,6},{2,0},{4,2},{6,4},{1,7},{3,1},{5,3},{7,5},{8,14},{10,8},{12,... | collective-permute-start | bytes 1572872 | tf_op jit(solution)/shard_map/ppermute | solution.py:19
  77.8 11.0 %collective-permute-done.16 = bf16[512,512]{1,0:T(8,128)(2,1)S(1)} collective-permute-done((bf16[512,512]{1,0:T(8,128)(2,1)S(1)}, bf16[512,512]{1,0:T(8,128)(2,1)S(1)}, u32[]{:S(2)}, u32[]{:S(2)}) %collective-permute-start.16) | collective-permute-done | bytes 524320 | tf_op jit(solution)/shard_map/ppermute | solution.py:19
  88.9 3.6 %collective-permute-start.17 = (bf16[256,512]{1,0:T(8,128)(2,1)S(1)}, bf16[256,512]{1,0:T(8,128)(2,1)S(1)}, u32[]{:S(2)}, u32[]{:S(2)}) collective-permute-start(bf16[256,512]{1,0:T(8,128)(2,1)S(1)} %add_convert_fusion.3), channel_id=1, source_target_pairs={{0,6},{2,0},{4,2},{6,4},{1,7},{3,1},{5,3},{7,5},{8,14},{10,8},{12,... | collective-permute-start | bytes 786440 | tf_op jit(solution)/shard_map/ppermute | solution.py:19
  92.6 4.4 %collective-permute-done.17 = bf16[256,512]{1,0:T(8,128)(2,1)S(1)} collective-permute-done((bf16[256,512]{1,0:T(8,128)(2,1)S(1)}, bf16[256,512]{1,0:T(8,128)(2,1)S(1)}, u32[]{:S(2)}, u32[]{:S(2)}) %collective-permute-start.17) | collective-permute-done | bytes 262176 | tf_op jit(solution)/shard_map/ppermute | solution.py:19
  97.1 3.4 %collective-permute-done.15 = bf16[256,512]{1,0:T(8,128)(2,1)S(1)} collective-permute-done((bf16[256,512]{1,0:T(8,128)(2,1)S(1)}, bf16[256,512]{1,0:T(8,128)(2,1)S(1)}, u32[]{:S(2)}, u32[]{:S(2)}) %collective-permute-start.15) | collective-permute-done | bytes 262176 | tf_op jit(solution)/shard_map/ppermute | solution.py:19
  100.8 2.7 %collective-permute-start.19 = (bf16[512,512]{1,0:T(8,128)(2,1)S(1)}, bf16[512,512]{1,0:T(8,128)(2,1)S(1)}, u32[]{:S(2)}, u32[]{:S(2)}) collective-permute-start(bf16[512,512]{1,0:T(8,128)(2,1)S(1)} %pad_maximum_fusion.1.m_own), channel_id=1, source_target_pairs={{0,6},{2,0},{4,2},{6,4},{1,7},{3,1},{5,3},{7,5},{8,14},{10,8},{12,... | collective-permute-start | bytes 1572872 | tf_op jit(solution)/shard_map/ppermute | solution.py:19
  103.5 10.0 %collective-permute-done.18.m_left = bf16[512,512]{1,0:T(8,128)(2,1)S(1)} collective-permute-done((bf16[512,512]{1,0:T(8,128)(2,1)S(1)}, bf16[512,512]{1,0:T(8,128)(2,1)S(1)}, u32[]{:S(2)}, u32[]{:S(2)}) %collective-permute-start.18) | collective-permute-done | bytes 524320 | tf_op jit(solution)/shard_map/ppermute | solution.py:19
  113.5 2.1 %all-gather.2.cloned.1.call-done.arrived = bf16[2048,2176]{1,0:T(8,128)(2,1)} async-done(((bf16[64,2176]{1,0:T(8,128)(2,1)}), bf16[2048,2176]{1,0:T(8,128)(2,1)}) %all-gather.2.cloned.1.call-update) | async-done | bytes 8912912 | tf_op jit(solution)/shard_map/all_gather | solution.py:249
  116.4 1.2 collective-permute-start.20
  118.3 1.5 collective-permute-start.21
  120.5 1.0 pad_maximum_fusion.t_far
  121.5 2.9 %collective-permute-done.20.m_low = bf16[256,512]{1,0:T(8,128)(2,1)} collective-permute-done((bf16[256,512]{1,0:T(8,128)(2,1)}, bf16[256,512]{1,0:T(8,128)(2,1)}, u32[]{:S(2)}, u32[]{:S(2)}) %collective-permute-start.20) | collective-permute-done | bytes 262176 | tf_op jit(solution)/shard_map/ppermute | solution.py:19
  125.5 5.5 %shard_map.129 = (bf16[512,2048]{1,0:T(8,128)(2,1)S(1)}, bf16[512,512]{1,0:T(8,128)(2,1)S(1)}, bf16[2048,2176]{1,0:T(8,128)(2,1)S(1)}) custom-call(s32[3]{0:T(128)S(1)} %copy-done.4, bf16[544,512]{1,0:T(8,128)(2,1)S(1)} %maximum_select_fusion.own.t_own, bf16[544,512]{1,0:T(8,128)(2,1)S(1)} %collective-permute-done.1.left.t_left, ...), custom_call_target="tpu_custom_call" | custom-call | flops 30000000 | bytes 6500000 | tf_op jit(solution)/shard_map/pallas_call | solution.py:281
  131.0 2.8 %collective-permute-start.22 = (bf16[512,2048]{1,0:T(8,128)(2,1)S(1)}, bf16[512,2048]{1,0:T(8,128)(2,1)S(1)}, u32[]{:S(2)}, u32[]{:S(2)}) collective-permute-start(bf16[512,2048]{1,0:T(8,128)(2,1)S(1)} %get-tuple-element.45.normed), channel_id=1, source_target_pairs={{0,1},{1,0},{2,3},{3,2},{4,5},{5,4},{6,7},{7,6},{8,9},{9,8},{10,11... | collective-permute-start | bytes 6291464 | tf_op jit(solution)/shard_map/ppermute | solution.py:19
  133.8 3.8 %collective-permute-done.22.normed = bf16[512,2048]{1,0:T(8,128)(2,1)S(1)} collective-permute-done((bf16[512,2048]{1,0:T(8,128)(2,1)S(1)}, bf16[512,2048]{1,0:T(8,128)(2,1)S(1)}, u32[]{:S(2)}, u32[]{:S(2)}) %collective-permute-start.22) | collective-permute-done | bytes 2097184 | tf_op jit(solution)/shard_map/ppermute | solution.py:19
  137.6 5.8 %shard_map.131 = bf16[4,512,512]{2,1,0:T(8,128)(2,1)S(1)} custom-call(s32[3]{0:T(128)S(1)} %copy-done.4, bf16[512,2048]{1,0:T(8,128)(2,1)S(1)} %collective-permute-done.22.normed, bf16[2048,2176]{1,0:T(8,128)(2,1)S(1)} %get-tuple-element.46.weights), custom_call_target="tpu_custom_call" | custom-call | flops 4499999744 | bytes 13000000 | tf_op jit(solution)/shard_map/pallas_call | solution.py:305
  143.9 5.8 %shard_map.130 = bf16[4,512,512]{2,1,0:T(8,128)(2,1)S(1)} custom-call(s32[3]{0:T(128)S(1)} %copy-done.4, bf16[512,2048]{1,0:T(8,128)(2,1)S(1)} %get-tuple-element.45.normed, bf16[2048,2176]{1,0:T(8,128)(2,1)S(1)} %get-tuple-element.46.weights), custom_call_target="tpu_custom_call" | custom-call | flops 4499999744 | bytes 13000000 | tf_op jit(solution)/shard_map/pallas_call | solution.py:306
  150.4 1.3 collective-permute-start.24
  151.7 1.6 collective-permute-start.26
  153.3 11.8 %collective-permute-done.24 = bf16[512,512]{1,0:T(8,128)(2,1)S(1)} collective-permute-done((bf16[512,512]{1,0:T(8,128)(2,1)S(1)}, bf16[512,512]{1,0:T(8,128)(2,1)S(1)}, u32[]{:S(2)}, u32[]{:S(2)}) %collective-permute-start.24) | collective-permute-done | bytes 524320 | tf_op jit(solution)/shard_map/ppermute | solution.py:19
  166.0 2.0 %collective-permute-start.27 = (bf16[256,512]{1,0:T(8,128)(2,1)S(1)}, bf16[256,512]{1,0:T(8,128)(2,1)S(1)}, u32[]{:S(2)}, u32[]{:S(2)}) collective-permute-start(bf16[256,512]{1,0:T(8,128)(2,1)S(1)} %get-tuple-element.53), channel_id=1, source_target_pairs={{0,6},{2,0},{4,2},{6,4},{1,7},{3,1},{5,3},{7,5},{8,14},{10,8},{12,... | collective-permute-start | bytes 786440 | tf_op jit(solution)/shard_map/ppermute | solution.py:19
  168.0 5.4 %collective-permute-done.25 = bf16[256,512]{1,0:T(8,128)(2,1)S(1)} collective-permute-done((bf16[256,512]{1,0:T(8,128)(2,1)S(1)}, bf16[256,512]{1,0:T(8,128)(2,1)S(1)}, u32[]{:S(2)}, u32[]{:S(2)}) %collective-permute-start.25) | collective-permute-done | bytes 262176 | tf_op jit(solution)/shard_map/ppermute | solution.py:19
  174.3 3.7 %all-to-all-start.1 = ((f32[4,4,128]{2,1,0:T(4,128)}), f32[4,4,128]{2,1,0:T(4,128)S(1)}, u32[]{:S(2)}, u32[]{:S(2)}) async-start(f32[4,4,128]{2,1,0:T(4,128)} %broadcast_in_dim.16), calls=%async_computation.1 | async-start | bytes 16384 | tf_op jit(solution)/shard_map/all_to_all | solution.py:317
  178.7 3.4 %all-to-all-done.1 = f32[4,4,128]{2,1,0:T(4,128)S(1)} async-done(((f32[4,4,128]{2,1,0:T(4,128)}), f32[4,4,128]{2,1,0:T(4,128)S(1)}, u32[]{:S(2)}, u32[]{:S(2)}) %all-to-all-start.1) | async-done | bytes 8224 | tf_op jit(solution)/shard_map/all_to_all | solution.py:317
  182.5 3.7 %collective-permute-start.28 = (bf16[512,256]{1,0:T(8,128)(2,1)S(1)}, bf16[512,256]{1,0:T(8,128)(2,1)S(1)}, u32[]{:S(2)}, u32[]{:S(2)}) collective-permute-start(bf16[512,256]{1,0:T(8,128)(2,1)S(1)} %get-tuple-element.60), channel_id=1, source_target_pairs={{0,1},{1,0},{2,3},{3,2},{4,5},{5,4},{6,7},{7,6},{8,9},{9,8},{10,11... | collective-permute-start | bytes 786440 | tf_op jit(solution)/shard_map/ppermute | solution.py:19
  186.2 1.2 collective-permute-done.28
  187.4 1.0 maximum_select_fusion.1
  (72 shorter events, 10.6 us)
Async XLA Ops:
  6.5 12.5 %copy-start.5 = (bf16[1024,256]{1,0:T(8,128)(2,1)S(1)}, bf16[1024,256]{1,0:T(8,128)(2,1)}, u32[]{:S(2)}) copy-start(bf16[1024,256]{1,0:T(8,128)(2,1)} %param.13) | copy-start | bytes 1572868
  6.5 109.1 %all-gather.2.cloned.1.call-start = ((), (), s32[]{:S(2)}) async-start(), calls=%async_computation.2 | async-start | bytes 9191424 | tf_op jit(solution)/shard_map/all_gather | solution.py:249
  10.0 28.5 %all-to-all-start = ((bf16[8,64,512]{2,1,0:T(8,128)(2,1)}), bf16[8,64,512]{2,1,0:T(8,128)(2,1)S(1)}, u32[]{:S(2)}, u32[]{:S(2)}) async-start(bf16[8,64,512]{2,1,0:T(8,128)(2,1)} %broadcast_in_dim.6), calls=%async_computation | async-start | bytes 1048576 | tf_op jit(solution)/shard_map/all_to_all | solution.py:34
  19.0 46.1 %copy-start.6 = (f32[2048]{0:T(1024)S(1)}, f32[2048]{0:T(1024)}, u32[]{:S(2)}) copy-start(f32[2048]{0:T(1024)} %param.14) | copy-start | bytes 24580
  19.1 2.2 %collective-permute-start = (bf16[544,256]{1,0:T(8,128)(2,1)S(1)}, bf16[544,256]{1,0:T(8,128)(2,1)S(1)}, u32[]{:S(2)}, u32[]{:S(2)}) collective-permute-start(bf16[544,256]{1,0:T(8,128)(2,1)S(1)} %get-tuple-element.64), channel_id=1, source_target_pairs={{0,1},{1,0},{2,3},{3,2},{4,5},{5,4},{6,7},{7,6},{8,9},{9,8},{10,11... | collective-permute-start | bytes 835592 | tf_op jit(solution)/shard_map/ppermute | solution.py:19
  21.4 20.2 %collective-permute-start.1 = (bf16[544,512]{1,0:T(8,128)(2,1)S(1)}, bf16[544,512]{1,0:T(8,128)(2,1)S(1)}, u32[]{:S(2)}, u32[]{:S(2)}) collective-permute-start(bf16[544,512]{1,0:T(8,128)(2,1)S(1)} %maximum_select_fusion.own.t_own), channel_id=1, source_target_pairs={{0,2},{2,4},{4,6},{6,0},{1,3},{3,5},{5,7},{7,1},{8,10},{10,12},{12... | collective-permute-start | bytes 1671176 | tf_op jit(solution)/shard_map/ppermute | solution.py:19
  22.7 18.9 %collective-permute-start.2 = (bf16[544,512]{1,0:T(8,128)(2,1)S(1)}, bf16[544,512]{1,0:T(8,128)(2,1)S(1)}, u32[]{:S(2)}, u32[]{:S(2)}) collective-permute-start(bf16[544,512]{1,0:T(8,128)(2,1)S(1)} %maximum_select_fusion.own.t_own), channel_id=1, source_target_pairs={{0,6},{2,0},{4,2},{6,4},{1,7},{3,1},{5,3},{7,5},{8,14},{10,8},{12,... | collective-permute-start | bytes 1671176 | tf_op jit(solution)/shard_map/ppermute | solution.py:19
  38.5 16.3 %collective-permute-start.5 = (bf16[8,64,512]{2,1,0:T(8,128)(2,1)S(1)}, bf16[8,64,512]{2,1,0:T(8,128)(2,1)S(1)}, u32[]{:S(2)}, u32[]{:S(2)}) collective-permute-start(bf16[8,64,512]{2,1,0:T(8,128)(2,1)S(1)} %all-to-all-done.rest_0_), channel_id=1, source_target_pairs={{0,8},{8,16},{16,24},{24,0},{1,9},{9,17},{17,25},{25,1},{2,10},{10... | collective-permute-start | bytes 1572872 | tf_op jit(solution)/shard_map/ppermute | solution.py:19
  40.0 14.8 %collective-permute-start.6 = (bf16[8,64,512]{2,1,0:T(8,128)(2,1)S(1)}, bf16[8,64,512]{2,1,0:T(8,128)(2,1)}, u32[]{:S(2)}, u32[]{:S(2)}) collective-permute-start(bf16[8,64,512]{2,1,0:T(8,128)(2,1)S(1)} %all-to-all-done.rest_0_), channel_id=1, source_target_pairs={{0,24},{8,0},{16,8},{24,16},{1,25},{9,1},{17,9},{25,17},{2,26},{10... | collective-permute-start | bytes 1572872 | tf_op jit(solution)/shard_map/ppermute | solution.py:19
  41.6 18.4 %collective-permute-start.3 = (bf16[288,512]{1,0:T(8,128)(2,1)S(1)}, bf16[288,512]{1,0:T(8,128)(2,1)S(1)}, u32[]{:S(2)}, u32[]{:S(2)}) collective-permute-start(bf16[288,512]{1,0:T(8,128)(2,1)S(1)} %slice.77), channel_id=1, source_target_pairs={{0,2},{2,4},{4,6},{6,0},{1,3},{3,5},{5,7},{7,1},{8,10},{10,12},{12... | collective-permute-start | bytes 884744 | tf_op jit(solution)/shard_map/ppermute | solution.py:19
  43.0 15.6 %collective-permute-start.4 = (bf16[256,512]{1,0:T(8,128)(2,1)S(1)}, bf16[256,512]{1,0:T(8,128)(2,1)S(1)}, u32[]{:S(2)}, u32[]{:S(2)}) collective-permute-start(bf16[256,512]{1,0:T(8,128)(2,1)S(1)} %slice.78), channel_id=1, source_target_pairs={{0,6},{2,0},{4,2},{6,4},{1,7},{3,1},{5,3},{7,5},{8,14},{10,8},{12,... | collective-permute-start | bytes 786440 | tf_op jit(solution)/shard_map/ppermute | solution.py:19
  44.5 21.4 %collective-permute-start.9 = (bf16[8,64,512]{2,1,0:T(8,128)(2,1)S(1)}, bf16[8,64,512]{2,1,0:T(8,128)(2,1)}, u32[]{:S(2)}, u32[]{:S(2)}) collective-permute-start(bf16[8,64,512]{2,1,0:T(8,128)(2,1)S(1)} %all-to-all-done.rest_0_), channel_id=1, source_target_pairs={{0,1},{1,0},{2,3},{3,2},{4,5},{5,4},{6,7},{7,6},{8,9},{9,8},{10,11... | collective-permute-start | bytes 1572872 | tf_op jit(solution)/shard_map/ppermute | solution.py:19
  54.8 8.3 %collective-permute-start.7 = (bf16[4,64,512]{2,1,0:T(8,128)(2,1)S(1)}, bf16[4,64,512]{2,1,0:T(8,128)(2,1)S(1)}, u32[]{:S(2)}, u32[]{:S(2)}) collective-permute-start(bf16[4,64,512]{2,1,0:T(8,128)(2,1)S(1)} %slice.79), channel_id=1, source_target_pairs={{0,8},{8,16},{16,24},{24,0},{1,9},{9,17},{17,25},{25,1},{2,10},{10... | collective-permute-start | bytes 786440 | tf_op jit(solution)/shard_map/ppermute | solution.py:19
  56.1 8.7 %collective-permute-start.8 = (bf16[4,64,512]{2,1,0:T(8,128)(2,1)S(1)}, bf16[4,64,512]{2,1,0:T(8,128)(2,1)}, u32[]{:S(2)}, u32[]{:S(2)}) collective-permute-start(bf16[4,64,512]{2,1,0:T(8,128)(2,1)S(1)} %slice.80), channel_id=1, source_target_pairs={{0,24},{8,0},{16,8},{24,16},{1,25},{9,1},{17,9},{25,17},{2,26},{10... | collective-permute-start | bytes 786440 | tf_op jit(solution)/shard_map/ppermute | solution.py:19
  58.6 16.5 %copy-start.2 = (bf16[256,512]{1,0:T(8,128)(2,1)}, bf16[256,512]{1,0:T(8,128)(2,1)S(1)}, u32[]{:S(2)}) copy-start(bf16[256,512]{1,0:T(8,128)(2,1)S(1)} %collective-permute-done.4.high) | copy-start | bytes 786436
  58.6 8.1 %collective-permute-start.10 = (bf16[8,64,512]{2,1,0:T(8,128)(2,1)S(1)}, bf16[8,64,512]{2,1,0:T(8,128)(2,1)}, u32[]{:S(2)}, u32[]{:S(2)}) collective-permute-start(bf16[8,64,512]{2,1,0:T(8,128)(2,1)S(1)} %collective-permute-done.5.rest_1_), channel_id=1, source_target_pairs={{0,1},{1,0},{2,3},{3,2},{4,5},{5,4},{6,7},{7,6},{8,9},{9,8},{10,11... | collective-permute-start | bytes 1572872 | tf_op jit(solution)/shard_map/ppermute | solution.py:19
  60.0 6.7 %collective-permute-start.11 = (bf16[8,64,512]{2,1,0:T(8,128)(2,1)}, bf16[8,64,512]{2,1,0:T(8,128)(2,1)}, u32[]{:S(2)}, u32[]{:S(2)}) collective-permute-start(bf16[8,64,512]{2,1,0:T(8,128)(2,1)} %collective-permute-done.6.rest_2_), channel_id=1, source_target_pairs={{0,1},{1,0},{2,3},{3,2},{4,5},{5,4},{6,7},{7,6},{8,9},{9,8},{10,11... | collective-permute-start | bytes 1572872 | tf_op jit(solution)/shard_map/ppermute | solution.py:19
  63.2 3.0 %collective-permute-start.12 = (bf16[4,64,512]{2,1,0:T(8,128)(2,1)S(1)}, bf16[4,64,512]{2,1,0:T(8,128)(2,1)}, u32[]{:S(2)}, u32[]{:S(2)}) collective-permute-start(bf16[4,64,512]{2,1,0:T(8,128)(2,1)S(1)} %collective-permute-done.7.rest_3_), channel_id=1, source_target_pairs={{0,1},{1,0},{2,3},{3,2},{4,5},{5,4},{6,7},{7,6},{8,9},{9,8},{10,11... | collective-permute-start | bytes 786440 | tf_op jit(solution)/shard_map/ppermute | solution.py:19
  64.8 1.9 collective-permute-start.13
  65.2 9.9 %copy-start.3 = (s32[3]{0:T(128)}, s32[3]{0:T(128)S(1)}, u32[]{:S(2)}) copy-start(s32[3]{0:T(128)S(1)} %pad_add_fusion.place) | copy-start | bytes 40
  75.1 13.7 %collective-permute-start.16 = (bf16[512,512]{1,0:T(8,128)(2,1)S(1)}, bf16[512,512]{1,0:T(8,128)(2,1)S(1)}, u32[]{:S(2)}, u32[]{:S(2)}) collective-permute-start(bf16[512,512]{1,0:T(8,128)(2,1)S(1)} %get-tuple-element.36), channel_id=1, source_target_pairs={{0,6},{2,0},{4,2},{6,4},{1,7},{3,1},{5,3},{7,5},{8,14},{10,8},{12,... | collective-permute-start | bytes 1572872 | tf_op jit(solution)/shard_map/ppermute | solution.py:19
  77.8 14.6 %collective-permute-start.14 = (bf16[512,512]{1,0:T(8,128)(2,1)S(1)}, bf16[512,512]{1,0:T(8,128)(2,1)S(1)}, u32[]{:S(2)}, u32[]{:S(2)}) collective-permute-start(bf16[512,512]{1,0:T(8,128)(2,1)S(1)} %get-tuple-element.34), channel_id=1, source_target_pairs={{0,2},{2,4},{4,6},{6,0},{1,3},{3,5},{5,7},{7,1},{8,10},{10,12},{12... | collective-permute-start | bytes 1572872 | tf_op jit(solution)/shard_map/ppermute | solution.py:19
  88.9 8.2 %collective-permute-start.17 = (bf16[256,512]{1,0:T(8,128)(2,1)S(1)}, bf16[256,512]{1,0:T(8,128)(2,1)S(1)}, u32[]{:S(2)}, u32[]{:S(2)}) collective-permute-start(bf16[256,512]{1,0:T(8,128)(2,1)S(1)} %add_convert_fusion.3), channel_id=1, source_target_pairs={{0,6},{2,0},{4,2},{6,4},{1,7},{3,1},{5,3},{7,5},{8,14},{10,8},{12,... | collective-permute-start | bytes 786440 | tf_op jit(solution)/shard_map/ppermute | solution.py:19
  92.6 7.9 %collective-permute-start.15 = (bf16[256,512]{1,0:T(8,128)(2,1)S(1)}, bf16[256,512]{1,0:T(8,128)(2,1)S(1)}, u32[]{:S(2)}, u32[]{:S(2)}) collective-permute-start(bf16[256,512]{1,0:T(8,128)(2,1)S(1)} %add_convert_fusion.4), channel_id=1, source_target_pairs={{0,2},{2,4},{4,6},{6,0},{1,3},{3,5},{5,7},{7,1},{8,10},{10,12},{12... | collective-permute-start | bytes 786440 | tf_op jit(solution)/shard_map/ppermute | solution.py:19
  100.5 19.3 %copy-start.7 = (f32[2048]{0:T(1024)S(1)}, f32[2048]{0:T(1024)}, u32[]{:S(2)}) copy-start(f32[2048]{0:T(1024)} %param.20) | copy-start | bytes 24580
  100.7 12.8 %collective-permute-start.18 = (bf16[512,512]{1,0:T(8,128)(2,1)S(1)}, bf16[512,512]{1,0:T(8,128)(2,1)S(1)}, u32[]{:S(2)}, u32[]{:S(2)}) collective-permute-start(bf16[512,512]{1,0:T(8,128)(2,1)S(1)} %pad_maximum_fusion.1.m_own), channel_id=1, source_target_pairs={{0,2},{2,4},{4,6},{6,0},{1,3},{3,5},{5,7},{7,1},{8,10},{10,12},{12... | collective-permute-start | bytes 1572872 | tf_op jit(solution)/shard_map/ppermute | solution.py:19
  100.8 12.7 %collective-permute-start.19 = (bf16[512,512]{1,0:T(8,128)(2,1)S(1)}, bf16[512,512]{1,0:T(8,128)(2,1)S(1)}, u32[]{:S(2)}, u32[]{:S(2)}) collective-permute-start(bf16[512,512]{1,0:T(8,128)(2,1)S(1)} %pad_maximum_fusion.1.m_own), channel_id=1, source_target_pairs={{0,6},{2,0},{4,2},{6,4},{1,7},{3,1},{5,3},{7,5},{8,14},{10,8},{12,... | collective-permute-start | bytes 1572872 | tf_op jit(solution)/shard_map/ppermute | solution.py:19
  116.4 8.0 %collective-permute-start.20 = (bf16[256,512]{1,0:T(8,128)(2,1)}, bf16[256,512]{1,0:T(8,128)(2,1)}, u32[]{:S(2)}, u32[]{:S(2)}) collective-permute-start(bf16[256,512]{1,0:T(8,128)(2,1)} %slice.87), channel_id=1, source_target_pairs={{0,2},{2,4},{4,6},{6,0},{1,3},{3,5},{5,7},{7,1},{8,10},{10,12},{12... | collective-permute-start | bytes 786440 | tf_op jit(solution)/shard_map/ppermute | solution.py:19
  118.3 6.5 %collective-permute-start.21 = (bf16[256,512]{1,0:T(8,128)(2,1)}, bf16[256,512]{1,0:T(8,128)(2,1)}, u32[]{:S(2)}, u32[]{:S(2)}) collective-permute-start(bf16[256,512]{1,0:T(8,128)(2,1)} %slice.88), channel_id=1, source_target_pairs={{0,6},{2,0},{4,2},{6,4},{1,7},{3,1},{5,3},{7,5},{8,14},{10,8},{12,... | collective-permute-start | bytes 786440 | tf_op jit(solution)/shard_map/ppermute | solution.py:19
  124.8 0.7 copy-start.4
  131.0 12.4 %copy-start = (bf16[512,512]{1,0:T(8,128)(2,1)}, bf16[512,512]{1,0:T(8,128)(2,1)S(1)}, u32[]{:S(2)}) copy-start(bf16[512,512]{1,0:T(8,128)(2,1)S(1)} %get-tuple-element.44) | copy-start | bytes 1572868
  131.0 6.6 %collective-permute-start.22 = (bf16[512,2048]{1,0:T(8,128)(2,1)S(1)}, bf16[512,2048]{1,0:T(8,128)(2,1)S(1)}, u32[]{:S(2)}, u32[]{:S(2)}) collective-permute-start(bf16[512,2048]{1,0:T(8,128)(2,1)S(1)} %get-tuple-element.45.normed), channel_id=1, source_target_pairs={{0,1},{1,0},{2,3},{3,2},{4,5},{5,4},{6,7},{7,6},{8,9},{9,8},{10,11... | collective-permute-start | bytes 6291464 | tf_op jit(solution)/shard_map/ppermute | solution.py:19
  143.4 6.2 %collective-permute-start.23 = (bf16[4,512,512]{2,1,0:T(8,128)(2,1)S(1)}, bf16[4,512,512]{2,1,0:T(8,128)(2,1)S(1)}, u32[]{:S(2)}, u32[]{:S(2)}) collective-permute-start(bf16[4,512,512]{2,1,0:T(8,128)(2,1)S(1)} %shard_map.131), channel_id=1, source_target_pairs={{0,1},{1,0},{2,3},{3,2},{4,5},{5,4},{6,7},{7,6},{8,9},{9,8},{10,11... | collective-permute-start | bytes 6291464 | tf_op jit(solution)/shard_map/ppermute | solution.py:19
  150.4 14.7 %collective-permute-start.24 = (bf16[512,512]{1,0:T(8,128)(2,1)S(1)}, bf16[512,512]{1,0:T(8,128)(2,1)S(1)}, u32[]{:S(2)}, u32[]{:S(2)}) collective-permute-start(bf16[512,512]{1,0:T(8,128)(2,1)S(1)} %pad_maximum_fusion.2), channel_id=1, source_target_pairs={{0,2},{2,4},{4,6},{6,0},{1,3},{3,5},{5,7},{7,1},{8,10},{10,12},{12... | collective-permute-start | bytes 1572872 | tf_op jit(solution)/shard_map/ppermute | solution.py:19
  151.7 30.5 %copy-start.1 = (bf16[512,512]{1,0:T(8,128)(2,1)S(1)}, bf16[512,512]{1,0:T(8,128)(2,1)}, u32[]{:S(2)}) copy-start(bf16[512,512]{1,0:T(8,128)(2,1)} %copy-done) | copy-start | bytes 1572868
  151.7 13.4 %collective-permute-start.26 = (bf16[512,512]{1,0:T(8,128)(2,1)S(1)}, bf16[512,512]{1,0:T(8,128)(2,1)S(1)}, u32[]{:S(2)}, u32[]{:S(2)}) collective-permute-start(bf16[512,512]{1,0:T(8,128)(2,1)S(1)} %pad_maximum_fusion.3), channel_id=1, source_target_pairs={{0,6},{2,0},{4,2},{6,4},{1,7},{3,1},{5,3},{7,5},{8,14},{10,8},{12,... | collective-permute-start | bytes 1572872 | tf_op jit(solution)/shard_map/ppermute | solution.py:19
  165.2 8.1 %collective-permute-start.25 = (bf16[256,512]{1,0:T(8,128)(2,1)S(1)}, bf16[256,512]{1,0:T(8,128)(2,1)S(1)}, u32[]{:S(2)}, u32[]{:S(2)}) collective-permute-start(bf16[256,512]{1,0:T(8,128)(2,1)S(1)} %get-tuple-element.54), channel_id=1, source_target_pairs={{0,2},{2,4},{4,6},{6,0},{1,3},{3,5},{5,7},{7,1},{8,10},{10,12},{12... | collective-permute-start | bytes 786440 | tf_op jit(solution)/shard_map/ppermute | solution.py:19
  166.0 7.3 %collective-permute-start.27 = (bf16[256,512]{1,0:T(8,128)(2,1)S(1)}, bf16[256,512]{1,0:T(8,128)(2,1)S(1)}, u32[]{:S(2)}, u32[]{:S(2)}) collective-permute-start(bf16[256,512]{1,0:T(8,128)(2,1)S(1)} %get-tuple-element.53), channel_id=1, source_target_pairs={{0,6},{2,0},{4,2},{6,4},{1,7},{3,1},{5,3},{7,5},{8,14},{10,8},{12,... | collective-permute-start | bytes 786440 | tf_op jit(solution)/shard_map/ppermute | solution.py:19
  174.3 7.8 %all-to-all-start.1 = ((f32[4,4,128]{2,1,0:T(4,128)}), f32[4,4,128]{2,1,0:T(4,128)S(1)}, u32[]{:S(2)}, u32[]{:S(2)}) async-start(f32[4,4,128]{2,1,0:T(4,128)} %broadcast_in_dim.16), calls=%async_computation.1 | async-start | bytes 16384 | tf_op jit(solution)/shard_map/all_to_all | solution.py:317
  182.5 4.9 %collective-permute-start.28 = (bf16[512,256]{1,0:T(8,128)(2,1)S(1)}, bf16[512,256]{1,0:T(8,128)(2,1)S(1)}, u32[]{:S(2)}, u32[]{:S(2)}) collective-permute-start(bf16[512,256]{1,0:T(8,128)(2,1)S(1)} %get-tuple-element.60), channel_id=1, source_target_pairs={{0,1},{1,0},{2,3},{3,2},{4,5},{5,4},{6,7},{7,6},{8,9},{9,8},{10,11... | collective-permute-start | bytes 786440 | tf_op jit(solution)/shard_map/ppermute | solution.py:19
Sparse Core Ops, SparseCore 0:
  9.9 105.6 all-gather.1
where the time goes:
time: 196 us; the launch traced here: 195 us
  waiting for transfers between devices  87.9 us (45%)
  starting transfers between devices  54.6 us (28%)
  Pallas kernels  27.2 us (14%)
  between operations  13.6 us (7%)
  local copies, waits for them, and re-layouts  6.28 us (3%)
  other arithmetic  5.53 us (3%)
    ppermute x29, waiting for transfers between devices, shift(): return lax.ppermute(value, axis, [(i, (i + by) % n) for i in range(n)])  68 us
    ppermute x29, starting transfers between devices, shift(): return lax.ppermute(value, axis, [(i, (i + by) % n) for i in range(n)])  42 us
    all_to_all x1, waiting for transfers between devices, copy_for_each(): lax.all_to_all(jnp.broadcast_to(value[None], (n, *value.shape)), axis, 0,...  14.3 us
    all_to_all x1, starting transfers between devices, copy_for_each(): lax.all_to_all(jnp.broadcast_to(value[None], (n, *value.shape)), axis, 0,...  9 us
    pallas_call x1, Pallas kernels, shards(): pl.pallas_call(mixer_kernel, out_shape=SHARES, in_specs=[SM] + [VM] * 5 +...  8.4 us
    pallas_call x1, Pallas kernels, shards(): forward(place, shift(normed, 'tp_1', 1), second)  5.77 us
    pallas_call x1, Pallas kernels, shards(): ours = forward(place, normed, second).astype(F32) + theirs  5.77 us
    pallas_call x1, Pallas kernels, shards(): pl.pallas_call(norm_kernel, out_shape=[jax.ShapeDtypeStruct((512, 2048),...  5.49 us
  transfers between devices with their start and end apart: 32, of which 18 were waited for; matrix products, arithmetic and copies ran while one was open for 4% of the time, Pallas kernels for 7%

commit v1 on v0

--- a/solution.py
+++ b/solution.py
@@ -201,24 +201,34 @@
     out[:, 2048:2176] = jnp.concatenate([down[:, 640:704], jnp.zeros((64, 64), BF16)], axis=1)
 
 
-def forward_kernel(place, normed, weights, out):
+def forward_kernel(place, normed, mine, other, out, fetched, hidden, sem):
+    copy = pltpu.make_async_copy(other, fetched, sem)
+    copy.start()
     x = place[0]
     lane = lax.broadcasted_iota(jnp.int32, (256, 128), 1)
+    for c, weights in enumerate((mine, fetched)):
+        if c == 1:
+            copy.wait()
+
+        @pl.loop(0, 2)
+        def _(i):
+            r = pl.ds(pl.multiple_of(i * 256, 256), 256)
+            both = jnp.dot(normed[r, :], weights[:, 0:1408], preferred_element_type=F32)
+            gate, up, tail = both[:, 0:640], both[:, 640:1280], both[:, 1280:1408]
+            hidden[r, c * 768 : c * 768 + 640] = (gate / (1.0 + jnp.exp(-gate)) * up).astype(BF16)
+            last = tail / (1.0 + jnp.exp(-tail)) * pltpu.roll(tail, 64, 1)
+            hidden[r, c * 768 + 640 : (c + 1) * 768] = jnp.where(lane < 64, last, 0.0).astype(BF16)
 
     @pl.loop(0, 2)
     def _(i):
         r = pl.ds(pl.multiple_of(i * 256, 256), 256)
-        both = jnp.dot(normed[r, :], weights[:, 0:1408], preferred_element_type=F32)
-        gate, up, tail = both[:, 0:640], both[:, 640:1280], both[:, 1280:1408]
-        hidden = (gate / (1.0 + jnp.exp(-gate)) * up).astype(BF16)
-        other = pltpu.roll(tail, 64, 1)
-        last = jnp.where(lane < 64, tail / (1.0 + jnp.exp(-tail)) * other, 0.0)
-        hidden = jnp.concatenate([hidden, last.astype(BF16)], axis=1)
         for j in range(4):
             start = pl.multiple_of(lax.rem(x + j, 4) * 512, 512)
             for zz in range(2):
                 n = pl.ds(start + zz * 256, 256)
-                out[j, r, zz * 256 : (zz + 1) * 256] = dot_nt(hidden, weights[n, 1408:2176]).astype(BF16)
+                share = dot_nt(hidden[r, 0:768], mine[n, 1408:2176])
+                share += dot_nt(hidden[r, 768:1536], fetched[n, 1408:2176])
+                out[j, r, zz * 256 : (zz + 1) * 256] = share.astype(BF16)
 
 
 VM = pl.BlockSpec(memory_space=pltpu.VMEM)
@@ -276,6 +286,7 @@
         cost_estimate=pl.CostEstimate(flops=2_300_000_000, bytes_accessed=9_000_000, transcendentals=0),
     )(place, t_own, t_left, t_right, t_low, t_high, *near, *near_other, own_taps, mixer_gain.reshape(4, 512))
     merged = scatter_sum(*pieces)
+    second_other = shift(second, "tp_1", 1)
     *gathered, second = around(merged, "tp_0", second)
 
     normed, first, second = pl.pallas_call(
@@ -294,17 +305,19 @@
         place, t_own, t_left, t_right, jnp.concatenate([t_low, t_high], 0), *gathered,
         merge_gain.reshape(4, 512), channel_gain.reshape(4, 512), second,
     )
-    forward = pl.pallas_call(
+    ours = pl.pallas_call(
         forward_kernel,
         out_shape=jax.ShapeDtypeStruct((4, 512, 512), BF16),
-        in_specs=[SM] + [VM] * 2,
+        in_specs=[SM] + [VM] * 2 + [HB],
         out_specs=VM,
-        compiler_params=pltpu.CompilerParams(vmem_limit_bytes=20 * 2**20),
-        cost_estimate=pl.CostEstimate(flops=4_500_000_000, bytes_accessed=13_000_000, transcendentals=0),
-    )
-    theirs = shift(forward(place, shift(normed, "tp_1", 1), second), "tp_1", 1).astype(F32)
-    ours = forward(place, normed, second).astype(F32) + theirs
-    ours = ours.astype(BF16)
+        scratch_shapes=[
+            pltpu.VMEM((2048, 2176), BF16),
+            pltpu.VMEM((512, 1536), BF16),
+            pltpu.SemaphoreType.DMA,
+        ],
+        compiler_params=pltpu.CompilerParams(vmem_limit_bytes=34 * 2**20),
+        cost_estimate=pl.CostEstimate(flops=9_000_000_000, bytes_accessed=13_000_000, transcendentals=0),
+    )(place, normed, second, second_other)
     pieces = (
         ours[0],
         jnp.concatenate([ours[2, :256], ours[1, 256:]], 0),

time: 196 us -> 290 us (1.48)
  waiting for transfers between devices: 87.9 us -> 181 us
    all_gather x1, waiting for transfers between devices: 2.12 us -> 105 us  [shards(): second = lax.all_gather(second_weights, FS, axis=0, tiled=True)]
    all_to_all x1, waiting for transfers between devices: 14.3 us -> 6.68 us  [copy_for_each(): lax.all_to_all(jnp.broadcast_to(value[None], (n, *value.shape)), axis, 0,...]
    all_to_all x1, starting transfers between devices: 9 us -> 4.08 us  [copy_for_each(): lax.all_to_all(jnp.broadcast_to(value[None], (n, *value.shape)), axis, 0,...]
    ppermute x29 -> x28, starting transfers between devices: 42 us -> 45.6 us  [shift(): return lax.ppermute(value, axis, [(i, (i + by) % n) for i in range(n)])]
    ppermute x29 -> x28, waiting for transfers between devices: 68 us -> 65.6 us  [shift(): return lax.ppermute(value, axis, [(i, (i + by) % n) for i in range(n)])]
    pallas_call x2 -> x1, Pallas kernels: 11.5 us -> 11.8 us  [shards(): pl.pallas_call(forward_kernel, out_shape=jax.ShapeDtypeStruct((4, 512, 51...]
  transfers between devices with their start and end apart: 32 -> 31, of which waited for: 18 -> 19; matrix products, arithmetic and copies ran while one was open for 4% -> 3% of each run, Pallas kernels for 7% -> 5%
where the time goes in v1:
time: 290 us; the launch traced here: 289 us
  waiting for transfers between devices  181 us (62%)
  starting transfers between devices  53.7 us (19%)
  Pallas kernels  28.1 us (10%)
  between operations  13.6 us (5%)
  local copies, waits for them, and re-layouts  8.19 us (3%)
  other arithmetic  4.91 us (2%)
    all_gather x1, waiting for transfers between devices, shards(): second = lax.all_gather(second_weights, FS, axis=0, tiled=True)  105 us
    ppermute x28, waiting for transfers between devices, shift(): return lax.ppermute(value, axis, [(i, (i + by) % n) for i in range(n)])  65.6 us
    ppermute x28, starting transfers between devices, shift(): return lax.ppermute(value, axis, [(i, (i + by) % n) for i in range(n)])  45.6 us
    pallas_call x1, Pallas kernels, shards(): pl.pallas_call(forward_kernel, out_shape=jax.ShapeDtypeStruct((4, 512, 51...  11.8 us
    pallas_call x1, Pallas kernels, shards(): pl.pallas_call(mixer_kernel, out_shape=SHARES, in_specs=[SM] + [VM] * 5 +...  9.07 us
    all_to_all x1, waiting for transfers between devices, copy_for_each(): lax.all_to_all(jnp.broadcast_to(value[None], (n, *value.shape)), axis, 0,...  6.68 us
  transfers between devices with their start and end apart: 31, of which 19 were waited for; matrix products, arithmetic and copies ran while one was open for 3% of the time, Pallas kernels for 5%

profile of v1, /device:TPU:1, one launch (start us, length us, event | category | flops | bytes accessed | tf_op | source)
XLA Modules:
  0.0 289.4 jit_solution(8392748835012427596)
XLA Ops:
  6.5 1.8 shard_map.128
  8.3 105.2 %all-gather.2.cloned.1.call-done.arrived = bf16[2048,2176]{1,0:T(8,128)(2,1)} async-done(((bf16[64,2176]{1,0:T(8,128)(2,1)}), bf16[2048,2176]{1,0:T(8,128)(2,1)}) %all-gather.2.cloned.1.call-update) | async-done | bytes 8912912 | tf_op jit(solution)/shard_map/all_gather | solution.py:259
  113.5 1.4 collective-permute-start.22
  114.9 0.8 pad_maximum_fusion.5
  115.7 0.8 broadcast_in_dim.6
  116.5 4.1 %all-to-all-start = ((bf16[8,64,512]{2,1,0:T(8,128)(2,1)}), bf16[8,64,512]{2,1,0:T(8,128)(2,1)S(1)}, u32[]{:S(2)}, u32[]{:S(2)}) async-start(bf16[8,64,512]{2,1,0:T(8,128)(2,1)} %broadcast_in_dim.6), calls=%async_computation | async-start | bytes 1048576 | tf_op jit(solution)/shard_map/all_to_all | solution.py:34
  121.0 8.0 %collective-permute-done = bf16[544,256]{1,0:T(8,128)(2,1)S(1)} collective-permute-done((bf16[544,256]{1,0:T(8,128)(2,1)S(1)}, bf16[544,256]{1,0:T(8,128)(2,1)S(1)}, u32[]{:S(2)}, u32[]{:S(2)}) %collective-permute-start) | collective-permute-done | bytes 278560 | tf_op jit(solution)/shard_map/ppermute | solution.py:19
  129.2 1.3 collective-permute-start.1
  130.5 1.5 collective-permute-start.2
  131.9 6.7 %all-to-all-done.rest_0_ = bf16[8,64,512]{2,1,0:T(8,128)(2,1)S(1)} async-done(((bf16[8,64,512]{2,1,0:T(8,128)(2,1)}), bf16[8,64,512]{2,1,0:T(8,128)(2,1)S(1)}, u32[]{:S(2)}, u32[]{:S(2)}) %all-to-all-start) | async-done | bytes 524320 | tf_op jit(solution)/shard_map/all_to_all | solution.py:34
  138.6 2.7 collective-permute-start.6
  141.3 3.0 %collective-permute-done.1.left.t_left = bf16[544,512]{1,0:T(8,128)(2,1)S(1)} collective-permute-done((bf16[544,512]{1,0:T(8,128)(2,1)S(1)}, bf16[544,512]{1,0:T(8,128)(2,1)S(1)}, u32[]{:S(2)}, u32[]{:S(2)}) %collective-permute-start.1) | collective-permute-done | bytes 557088 | tf_op jit(solution)/shard_map/ppermute | solution.py:19
  144.3 1.2 collective-permute-start.9
  145.7 7.2 %collective-permute-done.5.rest_1_ = bf16[8,64,512]{2,1,0:T(8,128)(2,1)S(1)} collective-permute-done((bf16[8,64,512]{2,1,0:T(8,128)(2,1)S(1)}, bf16[8,64,512]{2,1,0:T(8,128)(2,1)S(1)}, u32[]{:S(2)}, u32[]{:S(2)}) %collective-permute-start.5) | collective-permute-done | bytes 524320 | tf_op jit(solution)/shard_map/ppermute | solution.py:19
  152.9 2.4 collective-permute-start.4
  155.4 1.0 slice.80
  156.4 3.3 %collective-permute-done.4.high = bf16[256,512]{1,0:T(8,128)(2,1)S(1)} collective-permute-done((bf16[256,512]{1,0:T(8,128)(2,1)S(1)}, bf16[256,512]{1,0:T(8,128)(2,1)S(1)}, u32[]{:S(2)}, u32[]{:S(2)}) %collective-permute-start.4) | collective-permute-done | bytes 262176 | tf_op jit(solution)/shard_map/ppermute | solution.py:19
  159.6 2.3 collective-permute-start.10
  161.9 0.8 copy-done.5
  162.8 2.5 collective-permute-start.12
  165.4 3.0 %collective-permute-start.13 = (bf16[4,64,512]{2,1,0:T(8,128)(2,1)}, bf16[4,64,512]{2,1,0:T(8,128)(2,1)}, u32[]{:S(2)}, u32[]{:S(2)}) collective-permute-start(bf16[4,64,512]{2,1,0:T(8,128)(2,1)} %collective-permute-done.8.rest_4_), channel_id=1, source_target_pairs={{0,1},{1,0},{2,3},{3,2},{4,5},{5,4},{6,7},{7,6},{8,9},{9,8},{10,11... | collective-permute-start | bytes 786440 | tf_op jit(solution)/shard_map/ppermute | solution.py:19
  170.0 1.0 copy-done.6
  171.0 9.1 %shard_map.127 = (bf16[512,512]{1,0:T(8,128)(2,1)S(1)}, bf16[512,512]{1,0:T(8,128)(2,1)S(1)}, bf16[512,512]{1,0:T(8,128)(2,1)S(1)}, bf16[256,512]{1,0:T(8,128)(2,1)S(1)}, bf16[256,512]{1,0:T(8,128)(2,1)S(1)}) custom-call(s32[3]{0:T(128)S(1)} %pad_add_fusion.place, bf16[544,512]{1,0:T(8,128)(2,1)S(1)} %maximum_select_fusion.own.t_own, ...), custom_call_target="tpu_custom_call" | custom-call | flops 2300000000 | bytes 9000000 | tf_op jit(solution)/shard_map/pallas_call | solution.py:272
  180.1 3.5 %collective-permute-start.16 = (bf16[512,512]{1,0:T(8,128)(2,1)S(1)}, bf16[512,512]{1,0:T(8,128)(2,1)S(1)}, u32[]{:S(2)}, u32[]{:S(2)}) collective-permute-start(bf16[512,512]{1,0:T(8,128)(2,1)S(1)} %get-tuple-element.36), channel_id=1, source_target_pairs={{0,6},{2,0},{4,2},{6,4},{1,7},{3,1},{5,3},{7,5},{8,14},{10,8},{12,... | collective-permute-start | bytes 1572872 | tf_op jit(solution)/shard_map/ppermute | solution.py:19
  183.6 10.9 %collective-permute-done.16 = bf16[512,512]{1,0:T(8,128)(2,1)S(1)} collective-permute-done((bf16[512,512]{1,0:T(8,128)(2,1)S(1)}, bf16[512,512]{1,0:T(8,128)(2,1)S(1)}, u32[]{:S(2)}, u32[]{:S(2)}) %collective-permute-start.16) | collective-permute-done | bytes 524320 | tf_op jit(solution)/shard_map/ppermute | solution.py:19
  194.6 3.5 %collective-permute-start.17 = (bf16[256,512]{1,0:T(8,128)(2,1)S(1)}, bf16[256,512]{1,0:T(8,128)(2,1)S(1)}, u32[]{:S(2)}, u32[]{:S(2)}) collective-permute-start(bf16[256,512]{1,0:T(8,128)(2,1)S(1)} %add_convert_fusion.2), channel_id=1, source_target_pairs={{0,6},{2,0},{4,2},{6,4},{1,7},{3,1},{5,3},{7,5},{8,14},{10,8},{12,... | collective-permute-start | bytes 786440 | tf_op jit(solution)/shard_map/ppermute | solution.py:19
  198.2 4.3 %collective-permute-done.17 = bf16[256,512]{1,0:T(8,128)(2,1)S(1)} collective-permute-done((bf16[256,512]{1,0:T(8,128)(2,1)S(1)}, bf16[256,512]{1,0:T(8,128)(2,1)S(1)}, u32[]{:S(2)}, u32[]{:S(2)}) %collective-permute-start.17) | collective-permute-done | bytes 262176 | tf_op jit(solution)/shard_map/ppermute | solution.py:19
  202.5 3.3 %collective-permute-done.15 = bf16[256,512]{1,0:T(8,128)(2,1)S(1)} collective-permute-done((bf16[256,512]{1,0:T(8,128)(2,1)S(1)}, bf16[256,512]{1,0:T(8,128)(2,1)S(1)}, u32[]{:S(2)}, u32[]{:S(2)}) %collective-permute-start.15) | collective-permute-done | bytes 262176 | tf_op jit(solution)/shard_map/ppermute | solution.py:19
  206.1 2.7 collective-permute-start.19
  208.8 9.6 %collective-permute-done.18.m_left = bf16[512,512]{1,0:T(8,128)(2,1)S(1)} collective-permute-done((bf16[512,512]{1,0:T(8,128)(2,1)S(1)}, bf16[512,512]{1,0:T(8,128)(2,1)S(1)}, u32[]{:S(2)}, u32[]{:S(2)}) %collective-permute-start.18) | collective-permute-done | bytes 524320 | tf_op jit(solution)/shard_map/ppermute | solution.py:19
  219.9 2.7 collective-permute-start.21
  223.3 1.0 pad_maximum_fusion.t_far
  224.2 1.6 collective-permute-done.20.m_low
  226.2 5.5 %shard_map.129 = (bf16[512,2048]{1,0:T(8,128)(2,1)S(1)}, bf16[512,512]{1,0:T(8,128)(2,1)S(1)}, bf16[2048,2176]{1,0:T(8,128)(2,1)S(1)}) custom-call(s32[3]{0:T(128)S(1)} %copy-done.4, bf16[544,512]{1,0:T(8,128)(2,1)S(1)} %maximum_select_fusion.own.t_own, bf16[544,512]{1,0:T(8,128)(2,1)S(1)} %collective-permute-done.1.left.t_left, ...), custom_call_target="tpu_custom_call" | custom-call | flops 30000000 | bytes 6500000 | tf_op jit(solution)/shard_map/pallas_call | solution.py:292
  231.7 0.8 copy-done
  232.5 11.8 %shard_map.130 = bf16[4,512,512]{2,1,0:T(8,128)(2,1)S(1)} custom-call(s32[3]{0:T(128)S(1)} %copy-done.4, bf16[512,2048]{1,0:T(8,128)(2,1)S(1)} %get-tuple-element.45.normed, bf16[2048,2176]{1,0:T(8,128)(2,1)S(1)} %get-tuple-element.46.mine, bf16[2048,2176]{1,0:T(8,128)(2,1)} %collective-permute-done.22.other), custom_call_target="tpu_custom_call" | custom-call | flops 8999999488 | bytes 13000000 | tf_op jit(solution)/shard_map/pallas_call | solution.py:308
  244.4 1.4 collective-permute-start.23
  245.8 1.9 collective-permute-start.25
  247.7 7.5 %collective-permute-done.23 = bf16[512,512]{1,0:T(8,128)(2,1)S(1)} collective-permute-done((bf16[512,512]{1,0:T(8,128)(2,1)S(1)}, bf16[512,512]{1,0:T(8,128)(2,1)S(1)}, u32[]{:S(2)}, u32[]{:S(2)}) %collective-permute-start.23) | collective-permute-done | bytes 524320 | tf_op jit(solution)/shard_map/ppermute | solution.py:19
  255.4 0.8 collective-permute-start.24
  256.1 2.0 collective-permute-start.26
  258.1 4.4 %collective-permute-done.24 = bf16[256,512]{1,0:T(8,128)(2,1)S(1)} collective-permute-done((bf16[256,512]{1,0:T(8,128)(2,1)S(1)}, bf16[256,512]{1,0:T(8,128)(2,1)S(1)}, u32[]{:S(2)}, u32[]{:S(2)}) %collective-permute-start.24) | collective-permute-done | bytes 262176 | tf_op jit(solution)/shard_map/ppermute | solution.py:19
  263.6 4.1 %all-to-all-start.1 = ((f32[4,4,128]{2,1,0:T(4,128)}), f32[4,4,128]{2,1,0:T(4,128)S(1)}, u32[]{:S(2)}, u32[]{:S(2)}) async-start(f32[4,4,128]{2,1,0:T(4,128)} %broadcast_in_dim.16), calls=%async_computation.1 | async-start | bytes 16384 | tf_op jit(solution)/shard_map/all_to_all | solution.py:330
  267.6 0.8 dynamic_slice.21
  268.4 3.4 %all-to-all-done.1 = f32[4,4,128]{2,1,0:T(4,128)S(1)} async-done(((f32[4,4,128]{2,1,0:T(4,128)}), f32[4,4,128]{2,1,0:T(4,128)S(1)}, u32[]{:S(2)}, u32[]{:S(2)}) %all-to-all-start.1) | async-done | bytes 8224 | tf_op jit(solution)/shard_map/all_to_all | solution.py:330
  272.1 8.3 %collective-permute-start.27 = (bf16[512,256]{1,0:T(8,128)(2,1)S(1)}, bf16[512,256]{1,0:T(8,128)(2,1)S(1)}, u32[]{:S(2)}, u32[]{:S(2)}) collective-permute-start(bf16[512,256]{1,0:T(8,128)(2,1)S(1)} %get-tuple-element.60), channel_id=1, source_target_pairs={{0,1},{1,0},{2,3},{3,2},{4,5},{5,4},{6,7},{7,6},{8,9},{9,8},{10,11... | collective-permute-start | bytes 786440 | tf_op jit(solution)/shard_map/ppermute | solution.py:19
  280.4 1.2 collective-permute-done.27
  281.6 1.0 maximum_select_fusion.1
  (72 shorter events, 7.2 us)
Async XLA Ops:
  6.5 107.0 %all-gather.2.cloned.1.call-start = ((), (), s32[]{:S(2)}) async-start(), calls=%async_computation.2 | async-start | bytes 9191424 | tf_op jit(solution)/shard_map/all_gather | solution.py:259
  8.3 112.3 %copy-start.7 = (bf16[1024,256]{1,0:T(8,128)(2,1)S(1)}, bf16[1024,256]{1,0:T(8,128)(2,1)}, u32[]{:S(2)}) copy-start(bf16[1024,256]{1,0:T(8,128)(2,1)} %param.13) | copy-start | bytes 1572868
  113.5 119.0 %collective-permute-start.22 = (bf16[2048,2176]{1,0:T(8,128)(2,1)}, bf16[2048,2176]{1,0:T(8,128)(2,1)}, u32[]{:S(2)}, u32[]{:S(2)}) collective-permute-start(bf16[2048,2176]{1,0:T(8,128)(2,1)} %all-gather.2.cloned.1.call-done.arrived), channel_id=1, source_target_pairs={{0,1},{1,0},{2,3},{3,2},{4,5},{5,4},{6,7},{7,6},{8,9},{9,8},{10,11... | collective-permute-start | bytes 26738696 | tf_op jit(solution)/shard_map/ppermute | solution.py:19
  116.5 22.1 %all-to-all-start = ((bf16[8,64,512]{2,1,0:T(8,128)(2,1)}), bf16[8,64,512]{2,1,0:T(8,128)(2,1)S(1)}, u32[]{:S(2)}, u32[]{:S(2)}) async-start(bf16[8,64,512]{2,1,0:T(8,128)(2,1)} %broadcast_in_dim.6), calls=%async_computation | async-start | bytes 1048576 | tf_op jit(solution)/shard_map/all_to_all | solution.py:34
  120.7 8.4 %collective-permute-start = (bf16[544,256]{1,0:T(8,128)(2,1)S(1)}, bf16[544,256]{1,0:T(8,128)(2,1)S(1)}, u32[]{:S(2)}, u32[]{:S(2)}) collective-permute-start(bf16[544,256]{1,0:T(8,128)(2,1)S(1)} %get-tuple-element.64), channel_id=1, source_target_pairs={{0,1},{1,0},{2,3},{3,2},{4,5},{5,4},{6,7},{7,6},{8,9},{9,8},{10,11... | collective-permute-start | bytes 835592 | tf_op jit(solution)/shard_map/ppermute | solution.py:19
  129.2 39.3 %copy-start.8 = (f32[2048]{0:T(1024)S(1)}, f32[2048]{0:T(1024)}, u32[]{:S(2)}) copy-start(f32[2048]{0:T(1024)} %param.14) | copy-start | bytes 24580
  129.2 15.1 %collective-permute-start.1 = (bf16[544,512]{1,0:T(8,128)(2,1)S(1)}, bf16[544,512]{1,0:T(8,128)(2,1)S(1)}, u32[]{:S(2)}, u32[]{:S(2)}) collective-permute-start(bf16[544,512]{1,0:T(8,128)(2,1)S(1)} %maximum_select_fusion.own.t_own), channel_id=1, source_target_pairs={{0,2},{2,4},{4,6},{6,0},{1,3},{3,5},{5,7},{7,1},{8,10},{10,12},{12... | collective-permute-start | bytes 1671176 | tf_op jit(solution)/shard_map/ppermute | solution.py:19
  130.5 15.1 %collective-permute-start.2 = (bf16[544,512]{1,0:T(8,128)(2,1)S(1)}, bf16[544,512]{1,0:T(8,128)(2,1)S(1)}, u32[]{:S(2)}, u32[]{:S(2)}) collective-permute-start(bf16[544,512]{1,0:T(8,128)(2,1)S(1)} %maximum_select_fusion.own.t_own), channel_id=1, source_target_pairs={{0,6},{2,0},{4,2},{6,4},{1,7},{3,1},{5,3},{7,5},{8,14},{10,8},{12,... | collective-permute-start | bytes 1671176 | tf_op jit(solution)/shard_map/ppermute | solution.py:19
  138.6 14.2 %collective-permute-start.5 = (bf16[8,64,512]{2,1,0:T(8,128)(2,1)S(1)}, bf16[8,64,512]{2,1,0:T(8,128)(2,1)S(1)}, u32[]{:S(2)}, u32[]{:S(2)}) collective-permute-start(bf16[8,64,512]{2,1,0:T(8,128)(2,1)S(1)} %all-to-all-done.rest_0_), channel_id=1, source_target_pairs={{0,8},{8,16},{16,24},{24,0},{1,9},{9,17},{17,25},{25,1},{2,10},{10... | collective-permute-start | bytes 1572872 | tf_op jit(solution)/shard_map/ppermute | solution.py:19
  138.6 16.6 %collective-permute-start.6 = (bf16[8,64,512]{2,1,0:T(8,128)(2,1)S(1)}, bf16[8,64,512]{2,1,0:T(8,128)(2,1)}, u32[]{:S(2)}, u32[]{:S(2)}) collective-permute-start(bf16[8,64,512]{2,1,0:T(8,128)(2,1)S(1)} %all-to-all-done.rest_0_), channel_id=1, source_target_pairs={{0,24},{8,0},{16,8},{24,16},{1,25},{9,1},{17,9},{25,17},{2,26},{10... | collective-permute-start | bytes 1572872 | tf_op jit(solution)/shard_map/ppermute | solution.py:19
  144.3 17.6 %collective-permute-start.9 = (bf16[8,64,512]{2,1,0:T(8,128)(2,1)S(1)}, bf16[8,64,512]{2,1,0:T(8,128)(2,1)S(1)}, u32[]{:S(2)}, u32[]{:S(2)}) collective-permute-start(bf16[8,64,512]{2,1,0:T(8,128)(2,1)S(1)} %all-to-all-done.rest_0_), channel_id=1, source_target_pairs={{0,1},{1,0},{2,3},{3,2},{4,5},{5,4},{6,7},{7,6},{8,9},{9,8},{10,11... | collective-permute-start | bytes 1572872 | tf_op jit(solution)/shard_map/ppermute | solution.py:19
  145.5 14.1 %collective-permute-start.3 = (bf16[288,512]{1,0:T(8,128)(2,1)S(1)}, bf16[288,512]{1,0:T(8,128)(2,1)S(1)}, u32[]{:S(2)}, u32[]{:S(2)}) collective-permute-start(bf16[288,512]{1,0:T(8,128)(2,1)S(1)} %slice.77), channel_id=1, source_target_pairs={{0,2},{2,4},{4,6},{6,0},{1,3},{3,5},{5,7},{7,1},{8,10},{10,12},{12... | collective-permute-start | bytes 884744 | tf_op jit(solution)/shard_map/ppermute | solution.py:19
  152.9 6.8 %collective-permute-start.4 = (bf16[256,512]{1,0:T(8,128)(2,1)S(1)}, bf16[256,512]{1,0:T(8,128)(2,1)S(1)}, u32[]{:S(2)}, u32[]{:S(2)}) collective-permute-start(bf16[256,512]{1,0:T(8,128)(2,1)S(1)} %slice.78), channel_id=1, source_target_pairs={{0,6},{2,0},{4,2},{6,4},{1,7},{3,1},{5,3},{7,5},{8,14},{10,8},{12,... | collective-permute-start | bytes 786440 | tf_op jit(solution)/shard_map/ppermute | solution.py:19
  155.3 7.6 %collective-permute-start.7 = (bf16[4,64,512]{2,1,0:T(8,128)(2,1)S(1)}, bf16[4,64,512]{2,1,0:T(8,128)(2,1)S(1)}, u32[]{:S(2)}, u32[]{:S(2)}) collective-permute-start(bf16[4,64,512]{2,1,0:T(8,128)(2,1)S(1)} %slice.79), channel_id=1, source_target_pairs={{0,8},{8,16},{16,24},{24,0},{1,9},{9,17},{17,25},{25,1},{2,10},{10... | collective-permute-start | bytes 786440 | tf_op jit(solution)/shard_map/ppermute | solution.py:19
  159.6 20.5 %copy-start.2 = (bf16[256,512]{1,0:T(8,128)(2,1)}, bf16[256,512]{1,0:T(8,128)(2,1)S(1)}, u32[]{:S(2)}) copy-start(bf16[256,512]{1,0:T(8,128)(2,1)S(1)} %collective-permute-done.4.high) | copy-start | bytes 786436
  159.6 5.8 %collective-permute-start.8 = (bf16[4,64,512]{2,1,0:T(8,128)(2,1)S(1)}, bf16[4,64,512]{2,1,0:T(8,128)(2,1)}, u32[]{:S(2)}, u32[]{:S(2)}) collective-permute-start(bf16[4,64,512]{2,1,0:T(8,128)(2,1)S(1)} %slice.80), channel_id=1, source_target_pairs={{0,24},{8,0},{16,8},{24,16},{1,25},{9,1},{17,9},{25,17},{2,26},{10... | collective-permute-start | bytes 786440 | tf_op jit(solution)/shard_map/ppermute | solution.py:19
  159.6 10.3 %collective-permute-start.10 = (bf16[8,64,512]{2,1,0:T(8,128)(2,1)S(1)}, bf16[8,64,512]{2,1,0:T(8,128)(2,1)}, u32[]{:S(2)}, u32[]{:S(2)}) collective-permute-start(bf16[8,64,512]{2,1,0:T(8,128)(2,1)S(1)} %collective-permute-done.5.rest_1_), channel_id=1, source_target_pairs={{0,1},{1,0},{2,3},{3,2},{4,5},{5,4},{6,7},{7,6},{8,9},{9,8},{10,11... | collective-permute-start | bytes 1572872 | tf_op jit(solution)/shard_map/ppermute | solution.py:19
  161.9 0.8 copy-start.5
  162.7 7.3 %collective-permute-start.11 = (bf16[8,64,512]{2,1,0:T(8,128)(2,1)}, bf16[8,64,512]{2,1,0:T(8,128)(2,1)}, u32[]{:S(2)}, u32[]{:S(2)}) collective-permute-start(bf16[8,64,512]{2,1,0:T(8,128)(2,1)} %collective-permute-done.6.rest_2_), channel_id=1, source_target_pairs={{0,1},{1,0},{2,3},{3,2},{4,5},{5,4},{6,7},{7,6},{8,9},{9,8},{10,11... | collective-permute-start | bytes 1572872 | tf_op jit(solution)/shard_map/ppermute | solution.py:19
  162.8 6.4 %collective-permute-start.12 = (bf16[4,64,512]{2,1,0:T(8,128)(2,1)S(1)}, bf16[4,64,512]{2,1,0:T(8,128)(2,1)}, u32[]{:S(2)}, u32[]{:S(2)}) collective-permute-start(bf16[4,64,512]{2,1,0:T(8,128)(2,1)S(1)} %collective-permute-done.7.rest_3_), channel_id=1, source_target_pairs={{0,1},{1,0},{2,3},{3,2},{4,5},{5,4},{6,7},{7,6},{8,9},{9,8},{10,11... | collective-permute-start | bytes 786440 | tf_op jit(solution)/shard_map/ppermute | solution.py:19
  165.4 4.5 %collective-permute-start.13 = (bf16[4,64,512]{2,1,0:T(8,128)(2,1)}, bf16[4,64,512]{2,1,0:T(8,128)(2,1)}, u32[]{:S(2)}, u32[]{:S(2)}) collective-permute-start(bf16[4,64,512]{2,1,0:T(8,128)(2,1)} %collective-permute-done.8.rest_4_), channel_id=1, source_target_pairs={{0,1},{1,0},{2,3},{3,2},{4,5},{5,4},{6,7},{7,6},{8,9},{9,8},{10,11... | collective-permute-start | bytes 786440 | tf_op jit(solution)/shard_map/ppermute | solution.py:19
  168.5 11.6 %copy-start.3 = (s32[3]{0:T(128)}, s32[3]{0:T(128)S(1)}, u32[]{:S(2)}) copy-start(s32[3]{0:T(128)S(1)} %pad_add_fusion.place) | copy-start | bytes 40
  169.9 1.0 copy-start.6
  180.1 14.4 %collective-permute-start.16 = (bf16[512,512]{1,0:T(8,128)(2,1)S(1)}, bf16[512,512]{1,0:T(8,128)(2,1)S(1)}, u32[]{:S(2)}, u32[]{:S(2)}) collective-permute-start(bf16[512,512]{1,0:T(8,128)(2,1)S(1)} %get-tuple-element.36), channel_id=1, source_target_pairs={{0,6},{2,0},{4,2},{6,4},{1,7},{3,1},{5,3},{7,5},{8,14},{10,8},{12,... | collective-permute-start | bytes 1572872 | tf_op jit(solution)/shard_map/ppermute | solution.py:19
  183.6 14.5 %collective-permute-start.14 = (bf16[512,512]{1,0:T(8,128)(2,1)S(1)}, bf16[512,512]{1,0:T(8,128)(2,1)S(1)}, u32[]{:S(2)}, u32[]{:S(2)}) collective-permute-start(bf16[512,512]{1,0:T(8,128)(2,1)S(1)} %get-tuple-element.34), channel_id=1, source_target_pairs={{0,2},{2,4},{4,6},{6,0},{1,3},{3,5},{5,7},{7,1},{8,10},{10,12},{12... | collective-permute-start | bytes 1572872 | tf_op jit(solution)/shard_map/ppermute | solution.py:19
  194.6 7.9 %collective-permute-start.17 = (bf16[256,512]{1,0:T(8,128)(2,1)S(1)}, bf16[256,512]{1,0:T(8,128)(2,1)S(1)}, u32[]{:S(2)}, u32[]{:S(2)}) collective-permute-start(bf16[256,512]{1,0:T(8,128)(2,1)S(1)} %add_convert_fusion.2), channel_id=1, source_target_pairs={{0,6},{2,0},{4,2},{6,4},{1,7},{3,1},{5,3},{7,5},{8,14},{10,8},{12,... | collective-permute-start | bytes 786440 | tf_op jit(solution)/shard_map/ppermute | solution.py:19
  198.1 7.6 %collective-permute-start.15 = (bf16[256,512]{1,0:T(8,128)(2,1)S(1)}, bf16[256,512]{1,0:T(8,128)(2,1)S(1)}, u32[]{:S(2)}, u32[]{:S(2)}) collective-permute-start(bf16[256,512]{1,0:T(8,128)(2,1)S(1)} %add_convert_fusion.3), channel_id=1, source_target_pairs={{0,2},{2,4},{4,6},{6,0},{1,3},{3,5},{5,7},{7,1},{8,10},{10,12},{12... | collective-permute-start | bytes 786440 | tf_op jit(solution)/shard_map/ppermute | solution.py:19
  206.0 16.6 %copy-start.9 = (f32[2048]{0:T(1024)S(1)}, f32[2048]{0:T(1024)}, u32[]{:S(2)}) copy-start(f32[2048]{0:T(1024)} %param.20) | copy-start | bytes 24580
  206.0 12.4 %collective-permute-start.18 = (bf16[512,512]{1,0:T(8,128)(2,1)S(1)}, bf16[512,512]{1,0:T(8,128)(2,1)S(1)}, u32[]{:S(2)}, u32[]{:S(2)}) collective-permute-start(bf16[512,512]{1,0:T(8,128)(2,1)S(1)} %pad_maximum_fusion.1.m_own), channel_id=1, source_target_pairs={{0,2},{2,4},{4,6},{6,0},{1,3},{3,5},{5,7},{7,1},{8,10},{10,12},{12... | collective-permute-start | bytes 1572872 | tf_op jit(solution)/shard_map/ppermute | solution.py:19
  206.1 12.3 %collective-permute-start.19 = (bf16[512,512]{1,0:T(8,128)(2,1)S(1)}, bf16[512,512]{1,0:T(8,128)(2,1)S(1)}, u32[]{:S(2)}, u32[]{:S(2)}) collective-permute-start(bf16[512,512]{1,0:T(8,128)(2,1)S(1)} %pad_maximum_fusion.1.m_own), channel_id=1, source_target_pairs={{0,6},{2,0},{4,2},{6,4},{1,7},{3,1},{5,3},{7,5},{8,14},{10,8},{12,... | collective-permute-start | bytes 1572872 | tf_op jit(solution)/shard_map/ppermute | solution.py:19
  219.1 6.7 %collective-permute-start.20 = (bf16[256,512]{1,0:T(8,128)(2,1)}, bf16[256,512]{1,0:T(8,128)(2,1)}, u32[]{:S(2)}, u32[]{:S(2)}) collective-permute-start(bf16[256,512]{1,0:T(8,128)(2,1)} %slice.87), channel_id=1, source_target_pairs={{0,2},{2,4},{4,6},{6,0},{1,3},{3,5},{5,7},{7,1},{8,10},{10,12},{12... | collective-permute-start | bytes 786440 | tf_op jit(solution)/shard_map/ppermute | solution.py:19
  219.9 6.3 %collective-permute-start.21 = (bf16[256,512]{1,0:T(8,128)(2,1)}, bf16[256,512]{1,0:T(8,128)(2,1)}, u32[]{:S(2)}, u32[]{:S(2)}) collective-permute-start(bf16[256,512]{1,0:T(8,128)(2,1)} %slice.88), channel_id=1, source_target_pairs={{0,6},{2,0},{4,2},{6,4},{1,7},{3,1},{5,3},{7,5},{8,14},{10,8},{12,... | collective-permute-start | bytes 786440 | tf_op jit(solution)/shard_map/ppermute | solution.py:19
  223.3 2.9 %copy-start.4 = (s32[3]{0:T(128)S(1)}, s32[3]{0:T(128)}, u32[]{:S(2)}) copy-start(s32[3]{0:T(128)} %copy-done.3) | copy-start | bytes 40
  231.7 0.8 copy-start
  244.4 10.9 %collective-permute-start.23 = (bf16[512,512]{1,0:T(8,128)(2,1)S(1)}, bf16[512,512]{1,0:T(8,128)(2,1)S(1)}, u32[]{:S(2)}, u32[]{:S(2)}) collective-permute-start(bf16[512,512]{1,0:T(8,128)(2,1)S(1)} %pad_maximum_fusion.2), channel_id=1, source_target_pairs={{0,2},{2,4},{4,6},{6,0},{1,3},{3,5},{5,7},{7,1},{8,10},{10,12},{12... | collective-permute-start | bytes 1572872 | tf_op jit(solution)/shard_map/ppermute | solution.py:19
  245.8 9.4 %collective-permute-start.25 = (bf16[512,512]{1,0:T(8,128)(2,1)S(1)}, bf16[512,512]{1,0:T(8,128)(2,1)S(1)}, u32[]{:S(2)}, u32[]{:S(2)}) collective-permute-start(bf16[512,512]{1,0:T(8,128)(2,1)S(1)} %pad_maximum_fusion.3), channel_id=1, source_target_pairs={{0,6},{2,0},{4,2},{6,4},{1,7},{3,1},{5,3},{7,5},{8,14},{10,8},{12,... | collective-permute-start | bytes 1572872 | tf_op jit(solution)/shard_map/ppermute | solution.py:19
  255.4 7.2 %collective-permute-start.24 = (bf16[256,512]{1,0:T(8,128)(2,1)S(1)}, bf16[256,512]{1,0:T(8,128)(2,1)S(1)}, u32[]{:S(2)}, u32[]{:S(2)}) collective-permute-start(bf16[256,512]{1,0:T(8,128)(2,1)S(1)} %get-tuple-element.54), channel_id=1, source_target_pairs={{0,2},{2,4},{4,6},{6,0},{1,3},{3,5},{5,7},{7,1},{8,10},{10,12},{12... | collective-permute-start | bytes 786440 | tf_op jit(solution)/shard_map/ppermute | solution.py:19
  256.1 15.7 %copy-start.1 = (bf16[512,512]{1,0:T(8,128)(2,1)S(1)}, bf16[512,512]{1,0:T(8,128)(2,1)}, u32[]{:S(2)}) copy-start(bf16[512,512]{1,0:T(8,128)(2,1)} %copy-done) | copy-start | bytes 1572868
  256.1 6.4 %collective-permute-start.26 = (bf16[256,512]{1,0:T(8,128)(2,1)S(1)}, bf16[256,512]{1,0:T(8,128)(2,1)S(1)}, u32[]{:S(2)}, u32[]{:S(2)}) collective-permute-start(bf16[256,512]{1,0:T(8,128)(2,1)S(1)} %get-tuple-element.53), channel_id=1, source_target_pairs={{0,6},{2,0},{4,2},{6,4},{1,7},{3,1},{5,3},{7,5},{8,14},{10,8},{12,... | collective-permute-start | bytes 786440 | tf_op jit(solution)/shard_map/ppermute | solution.py:19
  263.6 8.2 %all-to-all-start.1 = ((f32[4,4,128]{2,1,0:T(4,128)}), f32[4,4,128]{2,1,0:T(4,128)S(1)}, u32[]{:S(2)}, u32[]{:S(2)}) async-start(f32[4,4,128]{2,1,0:T(4,128)} %broadcast_in_dim.16), calls=%async_computation.1 | async-start | bytes 16384 | tf_op jit(solution)/shard_map/all_to_all | solution.py:330
  272.1 9.4 %collective-permute-start.27 = (bf16[512,256]{1,0:T(8,128)(2,1)S(1)}, bf16[512,256]{1,0:T(8,128)(2,1)S(1)}, u32[]{:S(2)}, u32[]{:S(2)}) collective-permute-start(bf16[512,256]{1,0:T(8,128)(2,1)S(1)} %get-tuple-element.60), channel_id=1, source_target_pairs={{0,1},{1,0},{2,3},{3,2},{4,5},{5,4},{6,7},{7,6},{8,9},{9,8},{10,11... | collective-permute-start | bytes 786440 | tf_op jit(solution)/shard_map/ppermute | solution.py:19
Sparse Core Ops, SparseCore 0:
  9.9 103.5 all-gather.1

commit v2 on v1

--- a/solution.py
+++ b/solution.py
@@ -87,16 +87,8 @@
     for side in range(2):
         slot = k if side == 0 else 1 - k
         for q, (turn, begin, end) in enumerate(PARTS_Y):
-            at = lax.rem(y + turn, 4)
-            for b in range(begin, end):
-                row = pl.multiple_of((b * 4 + at) * 64, 64)
-                copies.append(
-                    pltpu.make_async_copy(
-                        pieces[side * 5 + q].at[b - begin],
-                        weights.at[slot, pl.ds(row, 64), :],
-                        sems.at[len(copies)],
-                    )
-                )
+            target = weights.at[slot, begin:end, lax.rem(y + turn, 4)]
+            copies.append(pltpu.make_async_copy(pieces[side * 5 + q], target, sems.at[len(copies)]))
     for copy in copies:
         copy.start()
     half = normed.shape[0] // 2
@@ -124,7 +116,7 @@
         at = pl.multiple_of(i * half, 16)
         for c in range(2):
             ch = slice(c * 128, (c + 1) * 128)
-            product = jnp.dot(normed[pl.ds(at, half), :], weights[c, :, 0:384], preferred_element_type=F32)
+            product = jnp.dot(normed[pl.ds(at, half), :], weights[c, :, :, :, 0:384].reshape(2048, 384), preferred_element_type=F32)
             outer[pl.ds(at, half), ch] = product[:, 0:128]
             signal[pl.ds(at + 8, half), ch] = product[:, 128:256] * product[:, 256:384]
 
@@ -145,8 +137,9 @@
     for j in range(4):
         start = pl.multiple_of(positions[j] * 512, 512)
         for zz in range(2):
-            n = pl.ds(start + zz * 256, 256)
-            w = jnp.concatenate([weights[0, n, 384:512], weights[1, n, 384:512]], axis=1)
+            n = 2 * positions[j] + zz
+            w = [weights[c, n, :, :, 384:512].reshape(256, 128) for c in range(2)]
+            w = jnp.concatenate(w, axis=1)
             share = dot_nt(mixed[...], w).astype(BF16)
             cols = slice(zz * 256, (zz + 1) * 256)
             for h in range(2):
@@ -168,11 +161,11 @@
     base = pl.multiple_of(k * HALO, HALO)
     for i in range(2):
 
-        @pl.loop(0, 8)
+        @pl.loop(0, 4)
         def _(tile):
-            at = pl.multiple_of(tile * 32, 32)
-            r, h = pl.ds(i * 256 + at, 32), pl.ds(at, 32)
-            tr = pl.ds(base + i * 256 + at, 32)
+            at = pl.multiple_of(tile * 64, 64)
+            r, h = pl.ds(i * 256 + at, 64), pl.ds(at, 64)
+            tr = pl.ds(base + i * 256 + at, 64)
             merged = [b.astype(F32) for b in (m_own[r, :], m_right[r, :], (m_low if i == 0 else m_high)[h, :], m_left[r, :])]
             toks = [b[tr, :].astype(F32) for b in (t_own, t_right, t_far, t_left)]
             squares = sum(jnp.sum(f * f, axis=1, keepdims=True) for f in merged)
@@ -275,12 +268,12 @@
         in_specs=[SM] + [VM] * 5 + [HB] * 10 + [VM] * 2,
         out_specs=[VM] * 5,
         scratch_shapes=[
-            pltpu.VMEM((2, 2048, 512), BF16),
+            pltpu.VMEM((2, 8, 4, 64, 512), BF16),
             pltpu.VMEM((span, 2048), BF16),
             pltpu.VMEM((span, 256), F32),
             pltpu.VMEM((span + 8, 256), F32),
             pltpu.VMEM((512, 256), BF16),
-            pltpu.SemaphoreType.DMA((64,)),
+            pltpu.SemaphoreType.DMA((10,)),
         ],
         compiler_params=pltpu.CompilerParams(vmem_limit_bytes=26 * 2**20),
         cost_estimate=pl.CostEstimate(flops=2_300_000_000, bytes_accessed=9_000_000, transcendentals=0),
@@ -326,8 +319,8 @@
         ours[3, 256:],
     )
     down = scatter_sum(*pieces).astype(F32)
-    squares = jnp.sum(down * down, axis=1).reshape(1, 4, 128)
-    total = lax.all_to_all(jnp.broadcast_to(squares, (4, 4, 128)), "tp_0", 0, 0, tiled=True).sum(0)
+    squares = jnp.sum(down * down, axis=1).reshape(4, 128)
+    total = squares + shift(squares, "tp_0", 1) + shift(squares, "tp_0", -1) + shift(squares, "tp_0", 2)
     factor = lax.rsqrt(total.reshape(512, 1) / 2048 + EPS)
     own_gain = lax.dynamic_slice_in_dim(output_gain, x * 512, 512)
     result = (first.astype(F32) + down * factor * own_gain).astype(BF16)

time: 290 us -> 285 us (0.983)
  Pallas kernels: 28.1 us -> 24.2 us
    ppermute x28 -> x31, starting transfers between devices: 45.6 us -> 50.4 us  [shift(): return lax.ppermute(value, axis, [(i, (i + by) % n) for i in range(n)])]
    all_to_all x1 -> x0, starting transfers between devices: 4.07 us -> none  [shards(): lax.all_to_all(jnp.broadcast_to(squares, (4, 4, 128)), 'tp_0', 0, 0, tile...]
    all_to_all x1 -> x0, waiting for transfers between devices: 3.41 us -> none  [shards(): lax.all_to_all(jnp.broadcast_to(squares, (4, 4, 128)), 'tp_0', 0, 0, tile...]
    pallas_call x1, Pallas kernels: 9.07 us -> 6.08 us  [shards(): pl.pallas_call(mixer_kernel, out_shape=SHARES, in_specs=[SM] + [VM] * 5 +...]
    ppermute x28 -> x31, waiting for transfers between devices: 65.6 us -> 67.5 us  [shift(): return lax.ppermute(value, axis, [(i, (i + by) % n) for i in range(n)])]
  transfers between devices with their start and end apart: 31 -> 33, of which waited for: 19 -> 19; matrix products, arithmetic and copies ran while one was open for 3% -> 3% of each run, Pallas kernels for 5% -> 4%
where the time goes in v2:
time: 285 us; the launch traced here: 284 us
  waiting for transfers between devices  179 us (63%)
  starting transfers between devices  54.5 us (19%)
  Pallas kernels  24.2 us (8%)
  between operations  13.6 us (5%)
  local copies, waits for them, and re-layouts  7.6 us (3%)
  other arithmetic  4.9 us (2%)
    all_gather x1, waiting for transfers between devices, shards(): second = lax.all_gather(second_weights, FS, axis=0, tiled=True)  105 us
    ppermute x31, waiting for transfers between devices, shift(): return lax.ppermute(value, axis, [(i, (i + by) % n) for i in range(n)])  67.5 us
    ppermute x31, starting transfers between devices, shift(): return lax.ppermute(value, axis, [(i, (i + by) % n) for i in range(n)])  50.4 us
    pallas_call x1, Pallas kernels, shards(): pl.pallas_call(forward_kernel, out_shape=jax.ShapeDtypeStruct((4, 512, 51...  11.8 us
    all_to_all x1, waiting for transfers between devices, copy_for_each(): lax.all_to_all(jnp.broadcast_to(value[None], (n, *value.shape)), axis, 0,...  6.68 us
    pallas_call x1, Pallas kernels, shards(): pl.pallas_call(mixer_kernel, out_shape=SHARES, in_specs=[SM] + [VM] * 5 +...  6.08 us
  transfers between devices with their start and end apart: 33, of which 19 were waited for; matrix products, arithmetic and copies ran while one was open for 3% of the time, Pallas kernels for 4%

profile of v2, /device:TPU:1, one launch (start us, length us, event | category | flops | bytes accessed | tf_op | source)
XLA Modules:
  0.0 284.2 jit_solution(100216228783893266)
XLA Ops:
  6.5 1.8 shard_map.128
  8.3 105.2 %all-gather.2.cloned.1.call-done.arrived = bf16[2048,2176]{1,0:T(8,128)(2,1)} async-done(((bf16[64,2176]{1,0:T(8,128)(2,1)}), bf16[2048,2176]{1,0:T(8,128)(2,1)}) %all-gather.2.cloned.1.call-update) | async-done | bytes 8912912 | tf_op jit(solution)/shard_map/all_gather | solution.py:252
  113.5 1.4 collective-permute-start.22
  114.9 0.8 pad_maximum_fusion.5
  115.7 0.8 broadcast_in_dim.2
  116.5 4.1 %all-to-all-start = ((bf16[8,64,512]{2,1,0:T(8,128)(2,1)}), bf16[8,64,512]{2,1,0:T(8,128)(2,1)S(1)}, u32[]{:S(2)}, u32[]{:S(2)}) async-start(bf16[8,64,512]{2,1,0:T(8,128)(2,1)} %broadcast_in_dim.2), calls=%async_computation | async-start | bytes 1048576 | tf_op jit(solution)/shard_map/all_to_all | solution.py:34
  121.0 8.0 %collective-permute-done = bf16[544,256]{1,0:T(8,128)(2,1)S(1)} collective-permute-done((bf16[544,256]{1,0:T(8,128)(2,1)S(1)}, bf16[544,256]{1,0:T(8,128)(2,1)S(1)}, u32[]{:S(2)}, u32[]{:S(2)}) %collective-permute-start) | collective-permute-done | bytes 278560 | tf_op jit(solution)/shard_map/ppermute | solution.py:19
  129.2 1.3 collective-permute-start.1
  130.5 1.5 collective-permute-start.2
  131.9 6.7 %all-to-all-done.rest_0_ = bf16[8,64,512]{2,1,0:T(8,128)(2,1)S(1)} async-done(((bf16[8,64,512]{2,1,0:T(8,128)(2,1)}), bf16[8,64,512]{2,1,0:T(8,128)(2,1)S(1)}, u32[]{:S(2)}, u32[]{:S(2)}) %all-to-all-start) | async-done | bytes 524320 | tf_op jit(solution)/shard_map/all_to_all | solution.py:34
  138.6 2.7 collective-permute-start.6
  141.3 3.0 %collective-permute-done.1.left.t_left = bf16[544,512]{1,0:T(8,128)(2,1)S(1)} collective-permute-done((bf16[544,512]{1,0:T(8,128)(2,1)S(1)}, bf16[544,512]{1,0:T(8,128)(2,1)S(1)}, u32[]{:S(2)}, u32[]{:S(2)}) %collective-permute-start.1) | collective-permute-done | bytes 557088 | tf_op jit(solution)/shard_map/ppermute | solution.py:19
  144.3 1.2 collective-permute-start.9
  145.7 7.2 %collective-permute-done.5.rest_1_ = bf16[8,64,512]{2,1,0:T(8,128)(2,1)S(1)} collective-permute-done((bf16[8,64,512]{2,1,0:T(8,128)(2,1)S(1)}, bf16[8,64,512]{2,1,0:T(8,128)(2,1)S(1)}, u32[]{:S(2)}, u32[]{:S(2)}) %collective-permute-start.5) | collective-permute-done | bytes 524320 | tf_op jit(solution)/shard_map/ppermute | solution.py:19
  152.9 2.4 collective-permute-start.4
  155.4 1.0 slice.80
  156.4 3.3 %collective-permute-done.4.high = bf16[256,512]{1,0:T(8,128)(2,1)S(1)} collective-permute-done((bf16[256,512]{1,0:T(8,128)(2,1)S(1)}, bf16[256,512]{1,0:T(8,128)(2,1)S(1)}, u32[]{:S(2)}, u32[]{:S(2)}) %collective-permute-start.4) | collective-permute-done | bytes 262176 | tf_op jit(solution)/shard_map/ppermute | solution.py:19
  159.6 2.3 collective-permute-start.10
  161.9 0.8 copy-done.5
  162.8 2.5 collective-permute-start.12
  165.4 3.0 %collective-permute-start.13 = (bf16[4,64,512]{2,1,0:T(8,128)(2,1)}, bf16[4,64,512]{2,1,0:T(8,128)(2,1)}, u32[]{:S(2)}, u32[]{:S(2)}) collective-permute-start(bf16[4,64,512]{2,1,0:T(8,128)(2,1)} %collective-permute-done.8.rest_4_), channel_id=1, source_target_pairs={{0,1},{1,0},{2,3},{3,2},{4,5},{5,4},{6,7},{7,6},{8,9},{9,8},{10,11... | collective-permute-start | bytes 786440 | tf_op jit(solution)/shard_map/ppermute | solution.py:19
  170.0 1.0 copy-done.6
  171.0 6.1 %shard_map.127 = (bf16[512,512]{1,0:T(8,128)(2,1)S(1)}, bf16[512,512]{1,0:T(8,128)(2,1)S(1)}, bf16[512,512]{1,0:T(8,128)(2,1)S(1)}, bf16[256,512]{1,0:T(8,128)(2,1)S(1)}, bf16[256,512]{1,0:T(8,128)(2,1)S(1)}) custom-call(s32[3]{0:T(128)S(1)} %pad_add_fusion.place, bf16[544,512]{1,0:T(8,128)(2,1)S(1)} %maximum_select_fusion.own.t_own, ...), custom_call_target="tpu_custom_call" | custom-call | flops 2300000000 | bytes 9000000 | tf_op jit(solution)/shard_map/pallas_call | solution.py:265
  177.1 3.5 %collective-permute-start.16 = (bf16[512,512]{1,0:T(8,128)(2,1)S(1)}, bf16[512,512]{1,0:T(8,128)(2,1)S(1)}, u32[]{:S(2)}, u32[]{:S(2)}) collective-permute-start(bf16[512,512]{1,0:T(8,128)(2,1)S(1)} %get-tuple-element.36), channel_id=1, source_target_pairs={{0,6},{2,0},{4,2},{6,4},{1,7},{3,1},{5,3},{7,5},{8,14},{10,8},{12,... | collective-permute-start | bytes 1572872 | tf_op jit(solution)/shard_map/ppermute | solution.py:19
  180.6 10.9 %collective-permute-done.16 = bf16[512,512]{1,0:T(8,128)(2,1)S(1)} collective-permute-done((bf16[512,512]{1,0:T(8,128)(2,1)S(1)}, bf16[512,512]{1,0:T(8,128)(2,1)S(1)}, u32[]{:S(2)}, u32[]{:S(2)}) %collective-permute-start.16) | collective-permute-done | bytes 524320 | tf_op jit(solution)/shard_map/ppermute | solution.py:19
  191.6 3.5 %collective-permute-start.17 = (bf16[256,512]{1,0:T(8,128)(2,1)S(1)}, bf16[256,512]{1,0:T(8,128)(2,1)S(1)}, u32[]{:S(2)}, u32[]{:S(2)}) collective-permute-start(bf16[256,512]{1,0:T(8,128)(2,1)S(1)} %add_convert_fusion.2), channel_id=1, source_target_pairs={{0,6},{2,0},{4,2},{6,4},{1,7},{3,1},{5,3},{7,5},{8,14},{10,8},{12,... | collective-permute-start | bytes 786440 | tf_op jit(solution)/shard_map/ppermute | solution.py:19
  195.2 4.3 %collective-permute-done.17 = bf16[256,512]{1,0:T(8,128)(2,1)S(1)} collective-permute-done((bf16[256,512]{1,0:T(8,128)(2,1)S(1)}, bf16[256,512]{1,0:T(8,128)(2,1)S(1)}, u32[]{:S(2)}, u32[]{:S(2)}) %collective-permute-start.17) | collective-permute-done | bytes 262176 | tf_op jit(solution)/shard_map/ppermute | solution.py:19
  199.5 3.3 %collective-permute-done.15 = bf16[256,512]{1,0:T(8,128)(2,1)S(1)} collective-permute-done((bf16[256,512]{1,0:T(8,128)(2,1)S(1)}, bf16[256,512]{1,0:T(8,128)(2,1)S(1)}, u32[]{:S(2)}, u32[]{:S(2)}) %collective-permute-start.15) | collective-permute-done | bytes 262176 | tf_op jit(solution)/shard_map/ppermute | solution.py:19
  203.2 2.7 collective-permute-start.19
  205.8 9.7 %collective-permute-done.18.m_left = bf16[512,512]{1,0:T(8,128)(2,1)S(1)} collective-permute-done((bf16[512,512]{1,0:T(8,128)(2,1)S(1)}, bf16[512,512]{1,0:T(8,128)(2,1)S(1)}, u32[]{:S(2)}, u32[]{:S(2)}) %collective-permute-start.18) | collective-permute-done | bytes 524320 | tf_op jit(solution)/shard_map/ppermute | solution.py:19
  216.9 2.7 collective-permute-start.21
  220.3 1.0 pad_maximum_fusion.t_far
  221.3 1.6 collective-permute-done.20.m_low
  223.2 4.6 %shard_map.129 = (bf16[512,2048]{1,0:T(8,128)(2,1)S(1)}, bf16[512,512]{1,0:T(8,128)(2,1)S(1)}, bf16[2048,2176]{1,0:T(8,128)(2,1)S(1)}) custom-call(s32[3]{0:T(128)S(1)} %copy-done.4, bf16[544,512]{1,0:T(8,128)(2,1)S(1)} %maximum_select_fusion.own.t_own, bf16[544,512]{1,0:T(8,128)(2,1)S(1)} %collective-permute-done.1.left.t_left, ...), custom_call_target="tpu_custom_call" | custom-call | flops 30000000 | bytes 6500000 | tf_op jit(solution)/shard_map/pallas_call | solution.py:285
  227.8 0.8 copy-done
  228.6 11.8 %shard_map.130 = bf16[4,512,512]{2,1,0:T(8,128)(2,1)S(1)} custom-call(s32[3]{0:T(128)S(1)} %copy-done.4, bf16[512,2048]{1,0:T(8,128)(2,1)S(1)} %get-tuple-element.45.normed, bf16[2048,2176]{1,0:T(8,128)(2,1)S(1)} %get-tuple-element.46.mine, bf16[2048,2176]{1,0:T(8,128)(2,1)} %collective-permute-done.22.other), custom_call_target="tpu_custom_call" | custom-call | flops 8999999488 | bytes 13000000 | tf_op jit(solution)/shard_map/pallas_call | solution.py:301
  240.5 1.4 collective-permute-start.23
  242.0 1.9 collective-permute-start.25
  243.9 7.5 %collective-permute-done.23 = bf16[512,512]{1,0:T(8,128)(2,1)S(1)} collective-permute-done((bf16[512,512]{1,0:T(8,128)(2,1)S(1)}, bf16[512,512]{1,0:T(8,128)(2,1)S(1)}, u32[]{:S(2)}, u32[]{:S(2)}) %collective-permute-start.23) | collective-permute-done | bytes 524320 | tf_op jit(solution)/shard_map/ppermute | solution.py:19
  252.3 2.0 collective-permute-start.26
  254.3 4.4 %collective-permute-done.24 = bf16[256,512]{1,0:T(8,128)(2,1)S(1)} collective-permute-done((bf16[256,512]{1,0:T(8,128)(2,1)S(1)}, bf16[256,512]{1,0:T(8,128)(2,1)S(1)}, u32[]{:S(2)}, u32[]{:S(2)}) %collective-permute-start.24) | collective-permute-done | bytes 262176 | tf_op jit(solution)/shard_map/ppermute | solution.py:19
  259.1 1.3 collective-permute-start.27
  260.4 1.7 collective-permute-start.28
  262.1 1.3 collective-permute-start.29
  264.2 1.8 collective-permute-done.29
  266.3 8.8 %collective-permute-start.30 = (bf16[512,256]{1,0:T(8,128)(2,1)S(1)}, bf16[512,256]{1,0:T(8,128)(2,1)S(1)}, u32[]{:S(2)}, u32[]{:S(2)}) collective-permute-start(bf16[512,256]{1,0:T(8,128)(2,1)S(1)} %get-tuple-element.60), channel_id=1, source_target_pairs={{0,1},{1,0},{2,3},{3,2},{4,5},{5,4},{6,7},{7,6},{8,9},{9,8},{10,11... | collective-permute-start | bytes 786440 | tf_op jit(solution)/shard_map/ppermute | solution.py:19
  275.2 1.2 collective-permute-done.30
  276.3 1.0 maximum_select_fusion.1
  (74 shorter events, 8.1 us)
Async XLA Ops:
  6.5 107.0 %all-gather.2.cloned.1.call-start = ((), (), s32[]{:S(2)}) async-start(), calls=%async_computation.1 | async-start | bytes 9191424 | tf_op jit(solution)/shard_map/all_gather | solution.py:252
  8.3 112.3 %copy-start.7 = (bf16[1024,256]{1,0:T(8,128)(2,1)S(1)}, bf16[1024,256]{1,0:T(8,128)(2,1)}, u32[]{:S(2)}) copy-start(bf16[1024,256]{1,0:T(8,128)(2,1)} %param.13) | copy-start | bytes 1572868
  113.5 115.1 %collective-permute-start.22 = (bf16[2048,2176]{1,0:T(8,128)(2,1)}, bf16[2048,2176]{1,0:T(8,128)(2,1)}, u32[]{:S(2)}, u32[]{:S(2)}) collective-permute-start(bf16[2048,2176]{1,0:T(8,128)(2,1)} %all-gather.2.cloned.1.call-done.arrived), channel_id=1, source_target_pairs={{0,1},{1,0},{2,3},{3,2},{4,5},{5,4},{6,7},{7,6},{8,9},{9,8},{10,11... | collective-permute-start | bytes 26738696 | tf_op jit(solution)/shard_map/ppermute | solution.py:19
  116.5 22.1 %all-to-all-start = ((bf16[8,64,512]{2,1,0:T(8,128)(2,1)}), bf16[8,64,512]{2,1,0:T(8,128)(2,1)S(1)}, u32[]{:S(2)}, u32[]{:S(2)}) async-start(bf16[8,64,512]{2,1,0:T(8,128)(2,1)} %broadcast_in_dim.2), calls=%async_computation | async-start | bytes 1048576 | tf_op jit(solution)/shard_map/all_to_all | solution.py:34
  120.7 8.4 %collective-permute-start = (bf16[544,256]{1,0:T(8,128)(2,1)S(1)}, bf16[544,256]{1,0:T(8,128)(2,1)S(1)}, u32[]{:S(2)}, u32[]{:S(2)}) collective-permute-start(bf16[544,256]{1,0:T(8,128)(2,1)S(1)} %get-tuple-element.64), channel_id=1, source_target_pairs={{0,1},{1,0},{2,3},{3,2},{4,5},{5,4},{6,7},{7,6},{8,9},{9,8},{10,11... | collective-permute-start | bytes 835592 | tf_op jit(solution)/shard_map/ppermute | solution.py:19
  129.2 39.3 %copy-start.8 = (f32[2048]{0:T(1024)S(1)}, f32[2048]{0:T(1024)}, u32[]{:S(2)}) copy-start(f32[2048]{0:T(1024)} %param.14) | copy-start | bytes 24580
  129.2 15.1 %collective-permute-start.1 = (bf16[544,512]{1,0:T(8,128)(2,1)S(1)}, bf16[544,512]{1,0:T(8,128)(2,1)S(1)}, u32[]{:S(2)}, u32[]{:S(2)}) collective-permute-start(bf16[544,512]{1,0:T(8,128)(2,1)S(1)} %maximum_select_fusion.own.t_own), channel_id=1, source_target_pairs={{0,2},{2,4},{4,6},{6,0},{1,3},{3,5},{5,7},{7,1},{8,10},{10,12},{12... | collective-permute-start | bytes 1671176 | tf_op jit(solution)/shard_map/ppermute | solution.py:19
  130.5 15.1 %collective-permute-start.2 = (bf16[544,512]{1,0:T(8,128)(2,1)S(1)}, bf16[544,512]{1,0:T(8,128)(2,1)S(1)}, u32[]{:S(2)}, u32[]{:S(2)}) collective-permute-start(bf16[544,512]{1,0:T(8,128)(2,1)S(1)} %maximum_select_fusion.own.t_own), channel_id=1, source_target_pairs={{0,6},{2,0},{4,2},{6,4},{1,7},{3,1},{5,3},{7,5},{8,14},{10,8},{12,... | collective-permute-start | bytes 1671176 | tf_op jit(solution)/shard_map/ppermute | solution.py:19
  138.6 14.2 %collective-permute-start.5 = (bf16[8,64,512]{2,1,0:T(8,128)(2,1)S(1)}, bf16[8,64,512]{2,1,0:T(8,128)(2,1)S(1)}, u32[]{:S(2)}, u32[]{:S(2)}) collective-permute-start(bf16[8,64,512]{2,1,0:T(8,128)(2,1)S(1)} %all-to-all-done.rest_0_), channel_id=1, source_target_pairs={{0,8},{8,16},{16,24},{24,0},{1,9},{9,17},{17,25},{25,1},{2,10},{10... | collective-permute-start | bytes 1572872 | tf_op jit(solution)/shard_map/ppermute | solution.py:19
  138.6 16.6 %collective-permute-start.6 = (bf16[8,64,512]{2,1,0:T(8,128)(2,1)S(1)}, bf16[8,64,512]{2,1,0:T(8,128)(2,1)}, u32[]{:S(2)}, u32[]{:S(2)}) collective-permute-start(bf16[8,64,512]{2,1,0:T(8,128)(2,1)S(1)} %all-to-all-done.rest_0_), channel_id=1, source_target_pairs={{0,24},{8,0},{16,8},{24,16},{1,25},{9,1},{17,9},{25,17},{2,26},{10... | collective-permute-start | bytes 1572872 | tf_op jit(solution)/shard_map/ppermute | solution.py:19
  144.3 17.6 %collective-permute-start.9 = (bf16[8,64,512]{2,1,0:T(8,128)(2,1)S(1)}, bf16[8,64,512]{2,1,0:T(8,128)(2,1)S(1)}, u32[]{:S(2)}, u32[]{:S(2)}) collective-permute-start(bf16[8,64,512]{2,1,0:T(8,128)(2,1)S(1)} %all-to-all-done.rest_0_), channel_id=1, source_target_pairs={{0,1},{1,0},{2,3},{3,2},{4,5},{5,4},{6,7},{7,6},{8,9},{9,8},{10,11... | collective-permute-start | bytes 1572872 | tf_op jit(solution)/shard_map/ppermute | solution.py:19
  145.5 14.1 %collective-permute-start.3 = (bf16[288,512]{1,0:T(8,128)(2,1)S(1)}, bf16[288,512]{1,0:T(8,128)(2,1)S(1)}, u32[]{:S(2)}, u32[]{:S(2)}) collective-permute-start(bf16[288,512]{1,0:T(8,128)(2,1)S(1)} %slice.77), channel_id=1, source_target_pairs={{0,2},{2,4},{4,6},{6,0},{1,3},{3,5},{5,7},{7,1},{8,10},{10,12},{12... | collective-permute-start | bytes 884744 | tf_op jit(solution)/shard_map/ppermute | solution.py:19
  152.9 6.8 %collective-permute-start.4 = (bf16[256,512]{1,0:T(8,128)(2,1)S(1)}, bf16[256,512]{1,0:T(8,128)(2,1)S(1)}, u32[]{:S(2)}, u32[]{:S(2)}) collective-permute-start(bf16[256,512]{1,0:T(8,128)(2,1)S(1)} %slice.78), channel_id=1, source_target_pairs={{0,6},{2,0},{4,2},{6,4},{1,7},{3,1},{5,3},{7,5},{8,14},{10,8},{12,... | collective-permute-start | bytes 786440 | tf_op jit(solution)/shard_map/ppermute | solution.py:19
  155.3 7.6 %collective-permute-start.7 = (bf16[4,64,512]{2,1,0:T(8,128)(2,1)S(1)}, bf16[4,64,512]{2,1,0:T(8,128)(2,1)S(1)}, u32[]{:S(2)}, u32[]{:S(2)}) collective-permute-start(bf16[4,64,512]{2,1,0:T(8,128)(2,1)S(1)} %slice.79), channel_id=1, source_target_pairs={{0,8},{8,16},{16,24},{24,0},{1,9},{9,17},{17,25},{25,1},{2,10},{10... | collective-permute-start | bytes 786440 | tf_op jit(solution)/shard_map/ppermute | solution.py:19
  159.6 17.5 %copy-start.2 = (bf16[256,512]{1,0:T(8,128)(2,1)}, bf16[256,512]{1,0:T(8,128)(2,1)S(1)}, u32[]{:S(2)}) copy-start(bf16[256,512]{1,0:T(8,128)(2,1)S(1)} %collective-permute-done.4.high) | copy-start | bytes 786436
  159.6 5.8 %collective-permute-start.8 = (bf16[4,64,512]{2,1,0:T(8,128)(2,1)S(1)}, bf16[4,64,512]{2,1,0:T(8,128)(2,1)}, u32[]{:S(2)}, u32[]{:S(2)}) collective-permute-start(bf16[4,64,512]{2,1,0:T(8,128)(2,1)S(1)} %slice.80), channel_id=1, source_target_pairs={{0,24},{8,0},{16,8},{24,16},{1,25},{9,1},{17,9},{25,17},{2,26},{10... | collective-permute-start | bytes 786440 | tf_op jit(solution)/shard_map/ppermute | solution.py:19
  159.6 10.3 %collective-permute-start.10 = (bf16[8,64,512]{2,1,0:T(8,128)(2,1)S(1)}, bf16[8,64,512]{2,1,0:T(8,128)(2,1)}, u32[]{:S(2)}, u32[]{:S(2)}) collective-permute-start(bf16[8,64,512]{2,1,0:T(8,128)(2,1)S(1)} %collective-permute-done.5.rest_1_), channel_id=1, source_target_pairs={{0,1},{1,0},{2,3},{3,2},{4,5},{5,4},{6,7},{7,6},{8,9},{9,8},{10,11... | collective-permute-start | bytes 1572872 | tf_op jit(solution)/shard_map/ppermute | solution.py:19
  161.9 0.8 copy-start.5
  162.7 7.3 %collective-permute-start.11 = (bf16[8,64,512]{2,1,0:T(8,128)(2,1)}, bf16[8,64,512]{2,1,0:T(8,128)(2,1)}, u32[]{:S(2)}, u32[]{:S(2)}) collective-permute-start(bf16[8,64,512]{2,1,0:T(8,128)(2,1)} %collective-permute-done.6.rest_2_), channel_id=1, source_target_pairs={{0,1},{1,0},{2,3},{3,2},{4,5},{5,4},{6,7},{7,6},{8,9},{9,8},{10,11... | collective-permute-start | bytes 1572872 | tf_op jit(solution)/shard_map/ppermute | solution.py:19
  162.8 6.4 %collective-permute-start.12 = (bf16[4,64,512]{2,1,0:T(8,128)(2,1)S(1)}, bf16[4,64,512]{2,1,0:T(8,128)(2,1)}, u32[]{:S(2)}, u32[]{:S(2)}) collective-permute-start(bf16[4,64,512]{2,1,0:T(8,128)(2,1)S(1)} %collective-permute-done.7.rest_3_), channel_id=1, source_target_pairs={{0,1},{1,0},{2,3},{3,2},{4,5},{5,4},{6,7},{7,6},{8,9},{9,8},{10,11... | collective-permute-start | bytes 786440 | tf_op jit(solution)/shard_map/ppermute | solution.py:19
  165.4 4.5 %collective-permute-start.13 = (bf16[4,64,512]{2,1,0:T(8,128)(2,1)}, bf16[4,64,512]{2,1,0:T(8,128)(2,1)}, u32[]{:S(2)}, u32[]{:S(2)}) collective-permute-start(bf16[4,64,512]{2,1,0:T(8,128)(2,1)} %collective-permute-done.8.rest_4_), channel_id=1, source_target_pairs={{0,1},{1,0},{2,3},{3,2},{4,5},{5,4},{6,7},{7,6},{8,9},{9,8},{10,11... | collective-permute-start | bytes 786440 | tf_op jit(solution)/shard_map/ppermute | solution.py:19
  168.5 8.6 %copy-start.3 = (s32[3]{0:T(128)}, s32[3]{0:T(128)S(1)}, u32[]{:S(2)}) copy-start(s32[3]{0:T(128)S(1)} %pad_add_fusion.place) | copy-start | bytes 40
  169.9 1.0 copy-start.6
  177.1 14.4 %collective-permute-start.16 = (bf16[512,512]{1,0:T(8,128)(2,1)S(1)}, bf16[512,512]{1,0:T(8,128)(2,1)S(1)}, u32[]{:S(2)}, u32[]{:S(2)}) collective-permute-start(bf16[512,512]{1,0:T(8,128)(2,1)S(1)} %get-tuple-element.36), channel_id=1, source_target_pairs={{0,6},{2,0},{4,2},{6,4},{1,7},{3,1},{5,3},{7,5},{8,14},{10,8},{12,... | collective-permute-start | bytes 1572872 | tf_op jit(solution)/shard_map/ppermute | solution.py:19
  180.6 14.5 %collective-permute-start.14 = (bf16[512,512]{1,0:T(8,128)(2,1)S(1)}, bf16[512,512]{1,0:T(8,128)(2,1)S(1)}, u32[]{:S(2)}, u32[]{:S(2)}) collective-permute-start(bf16[512,512]{1,0:T(8,128)(2,1)S(1)} %get-tuple-element.34), channel_id=1, source_target_pairs={{0,2},{2,4},{4,6},{6,0},{1,3},{3,5},{5,7},{7,1},{8,10},{10,12},{12... | collective-permute-start | bytes 1572872 | tf_op jit(solution)/shard_map/ppermute | solution.py:19
  191.6 7.9 %collective-permute-start.17 = (bf16[256,512]{1,0:T(8,128)(2,1)S(1)}, bf16[256,512]{1,0:T(8,128)(2,1)S(1)}, u32[]{:S(2)}, u32[]{:S(2)}) collective-permute-start(bf16[256,512]{1,0:T(8,128)(2,1)S(1)} %add_convert_fusion.2), channel_id=1, source_target_pairs={{0,6},{2,0},{4,2},{6,4},{1,7},{3,1},{5,3},{7,5},{8,14},{10,8},{12,... | collective-permute-start | bytes 786440 | tf_op jit(solution)/shard_map/ppermute | solution.py:19
  195.1 7.7 %collective-permute-start.15 = (bf16[256,512]{1,0:T(8,128)(2,1)S(1)}, bf16[256,512]{1,0:T(8,128)(2,1)S(1)}, u32[]{:S(2)}, u32[]{:S(2)}) collective-permute-start(bf16[256,512]{1,0:T(8,128)(2,1)S(1)} %add_convert_fusion.3), channel_id=1, source_target_pairs={{0,2},{2,4},{4,6},{6,0},{1,3},{3,5},{5,7},{7,1},{8,10},{10,12},{12... | collective-permute-start | bytes 786440 | tf_op jit(solution)/shard_map/ppermute | solution.py:19
  203.0 16.6 %copy-start.9 = (f32[2048]{0:T(1024)S(1)}, f32[2048]{0:T(1024)}, u32[]{:S(2)}) copy-start(f32[2048]{0:T(1024)} %param.20) | copy-start | bytes 24580
  203.1 12.4 %collective-permute-start.18 = (bf16[512,512]{1,0:T(8,128)(2,1)S(1)}, bf16[512,512]{1,0:T(8,128)(2,1)S(1)}, u32[]{:S(2)}, u32[]{:S(2)}) collective-permute-start(bf16[512,512]{1,0:T(8,128)(2,1)S(1)} %pad_maximum_fusion.1.m_own), channel_id=1, source_target_pairs={{0,2},{2,4},{4,6},{6,0},{1,3},{3,5},{5,7},{7,1},{8,10},{10,12},{12... | collective-permute-start | bytes 1572872 | tf_op jit(solution)/shard_map/ppermute | solution.py:19
  203.2 12.3 %collective-permute-start.19 = (bf16[512,512]{1,0:T(8,128)(2,1)S(1)}, bf16[512,512]{1,0:T(8,128)(2,1)S(1)}, u32[]{:S(2)}, u32[]{:S(2)}) collective-permute-start(bf16[512,512]{1,0:T(8,128)(2,1)S(1)} %pad_maximum_fusion.1.m_own), channel_id=1, source_target_pairs={{0,6},{2,0},{4,2},{6,4},{1,7},{3,1},{5,3},{7,5},{8,14},{10,8},{12,... | collective-permute-start | bytes 1572872 | tf_op jit(solution)/shard_map/ppermute | solution.py:19
  216.2 6.7 %collective-permute-start.20 = (bf16[256,512]{1,0:T(8,128)(2,1)}, bf16[256,512]{1,0:T(8,128)(2,1)}, u32[]{:S(2)}, u32[]{:S(2)}) collective-permute-start(bf16[256,512]{1,0:T(8,128)(2,1)} %slice.87), channel_id=1, source_target_pairs={{0,2},{2,4},{4,6},{6,0},{1,3},{3,5},{5,7},{7,1},{8,10},{10,12},{12... | collective-permute-start | bytes 786440 | tf_op jit(solution)/shard_map/ppermute | solution.py:19
  216.9 6.3 %collective-permute-start.21 = (bf16[256,512]{1,0:T(8,128)(2,1)}, bf16[256,512]{1,0:T(8,128)(2,1)}, u32[]{:S(2)}, u32[]{:S(2)}) collective-permute-start(bf16[256,512]{1,0:T(8,128)(2,1)} %slice.88), channel_id=1, source_target_pairs={{0,6},{2,0},{4,2},{6,4},{1,7},{3,1},{5,3},{7,5},{8,14},{10,8},{12,... | collective-permute-start | bytes 786440 | tf_op jit(solution)/shard_map/ppermute | solution.py:19
  220.3 2.9 %copy-start.4 = (s32[3]{0:T(128)S(1)}, s32[3]{0:T(128)}, u32[]{:S(2)}) copy-start(s32[3]{0:T(128)} %copy-done.3) | copy-start | bytes 40
  227.8 0.8 copy-start
  240.5 10.9 %collective-permute-start.23 = (bf16[512,512]{1,0:T(8,128)(2,1)S(1)}, bf16[512,512]{1,0:T(8,128)(2,1)S(1)}, u32[]{:S(2)}, u32[]{:S(2)}) collective-permute-start(bf16[512,512]{1,0:T(8,128)(2,1)S(1)} %pad_maximum_fusion.2), channel_id=1, source_target_pairs={{0,2},{2,4},{4,6},{6,0},{1,3},{3,5},{5,7},{7,1},{8,10},{10,12},{12... | collective-permute-start | bytes 1572872 | tf_op jit(solution)/shard_map/ppermute | solution.py:19
  242.0 9.4 %collective-permute-start.25 = (bf16[512,512]{1,0:T(8,128)(2,1)S(1)}, bf16[512,512]{1,0:T(8,128)(2,1)S(1)}, u32[]{:S(2)}, u32[]{:S(2)}) collective-permute-start(bf16[512,512]{1,0:T(8,128)(2,1)S(1)} %pad_maximum_fusion.3), channel_id=1, source_target_pairs={{0,6},{2,0},{4,2},{6,4},{1,7},{3,1},{5,3},{7,5},{8,14},{10,8},{12,... | collective-permute-start | bytes 1572872 | tf_op jit(solution)/shard_map/ppermute | solution.py:19
  251.5 7.2 %collective-permute-start.24 = (bf16[256,512]{1,0:T(8,128)(2,1)S(1)}, bf16[256,512]{1,0:T(8,128)(2,1)S(1)}, u32[]{:S(2)}, u32[]{:S(2)}) collective-permute-start(bf16[256,512]{1,0:T(8,128)(2,1)S(1)} %get-tuple-element.54), channel_id=1, source_target_pairs={{0,2},{2,4},{4,6},{6,0},{1,3},{3,5},{5,7},{7,1},{8,10},{10,12},{12... | collective-permute-start | bytes 786440 | tf_op jit(solution)/shard_map/ppermute | solution.py:19
  252.3 13.7 %copy-start.1 = (bf16[512,512]{1,0:T(8,128)(2,1)S(1)}, bf16[512,512]{1,0:T(8,128)(2,1)}, u32[]{:S(2)}) copy-start(bf16[512,512]{1,0:T(8,128)(2,1)} %copy-done) | copy-start | bytes 1572868
  252.3 6.4 %collective-permute-start.26 = (bf16[256,512]{1,0:T(8,128)(2,1)S(1)}, bf16[256,512]{1,0:T(8,128)(2,1)S(1)}, u32[]{:S(2)}, u32[]{:S(2)}) collective-permute-start(bf16[256,512]{1,0:T(8,128)(2,1)S(1)} %get-tuple-element.53), channel_id=1, source_target_pairs={{0,6},{2,0},{4,2},{6,4},{1,7},{3,1},{5,3},{7,5},{8,14},{10,8},{12,... | collective-permute-start | bytes 786440 | tf_op jit(solution)/shard_map/ppermute | solution.py:19
  259.1 5.1 %collective-permute-start.27 = (f32[4,128]{1,0:T(4,128)S(1)}, f32[4,128]{1,0:T(4,128)S(1)}, u32[]{:S(2)}, u32[]{:S(2)}) collective-permute-start(f32[4,128]{1,0:T(4,128)S(1)} %bitcast.39), channel_id=1, source_target_pairs={{0,2},{2,4},{4,6},{6,0},{1,3},{3,5},{5,7},{7,1},{8,10},{10,12},{12... | collective-permute-start | bytes 6152 | tf_op jit(solution)/shard_map/ppermute | solution.py:19
  260.4 3.8 %collective-permute-start.28 = (f32[4,128]{1,0:T(4,128)S(1)}, f32[4,128]{1,0:T(4,128)S(1)}, u32[]{:S(2)}, u32[]{:S(2)}) collective-permute-start(f32[4,128]{1,0:T(4,128)S(1)} %bitcast.40), channel_id=1, source_target_pairs={{0,6},{2,0},{4,2},{6,4},{1,7},{3,1},{5,3},{7,5},{8,14},{10,8},{12,... | collective-permute-start | bytes 6152 | tf_op jit(solution)/shard_map/ppermute | solution.py:19
  262.1 3.9 %collective-permute-start.29 = (f32[4,128]{1,0:T(4,128)S(1)}, f32[4,128]{1,0:T(4,128)S(1)}, u32[]{:S(2)}, u32[]{:S(2)}) collective-permute-start(f32[4,128]{1,0:T(4,128)S(1)} %bitcast.41), channel_id=1, source_target_pairs={{0,4},{2,6},{4,0},{6,2},{1,5},{3,7},{5,1},{7,3},{8,12},{10,14},{12... | collective-permute-start | bytes 6152 | tf_op jit(solution)/shard_map/ppermute | solution.py:19
  266.3 10.0 %collective-permute-start.30 = (bf16[512,256]{1,0:T(8,128)(2,1)S(1)}, bf16[512,256]{1,0:T(8,128)(2,1)S(1)}, u32[]{:S(2)}, u32[]{:S(2)}) collective-permute-start(bf16[512,256]{1,0:T(8,128)(2,1)S(1)} %get-tuple-element.60), channel_id=1, source_target_pairs={{0,1},{1,0},{2,3},{3,2},{4,5},{5,4},{6,7},{7,6},{8,9},{9,8},{10,11... | collective-permute-start | bytes 786440 | tf_op jit(solution)/shard_map/ppermute | solution.py:19
Sparse Core Ops, SparseCore 0:
  9.9 103.5 all-gather.1

commit v3 on v2

--- a/solution.py
+++ b/solution.py
@@ -23,7 +23,8 @@
     half = cut or value.shape[0] // 2
     left = shift(value, axis, 1)
     right = shift(value, axis, -1)
-    left, right, *held = lax.optimization_barrier((left, right, *held))
+    if held:
+        left, right, *held = lax.optimization_barrier((left, right, *held))
     far_low = shift(left[:half], axis, 1)
     far_high = shift(right[half:], axis, -1)
     return value, left, right, far_low, far_high, *held
@@ -194,34 +195,44 @@
     out[:, 2048:2176] = jnp.concatenate([down[:, 640:704], jnp.zeros((64, 64), BF16)], axis=1)
 
 
-def forward_kernel(place, normed, mine, other, out, fetched, hidden, sem):
+def gate_rows(normed, weights, hidden):
+    lane = lax.broadcasted_iota(jnp.int32, (256, 128), 1)
+
+    @pl.loop(0, 2)
+    def _(i):
+        r = pl.ds(pl.multiple_of(i * 256, 256), 256)
+        both = jnp.dot(normed[r, :], weights[:, 0:1408], preferred_element_type=F32)
+        gate, up, tail = both[:, 0:640], both[:, 640:1280], both[:, 1280:1408]
+        hidden[r, 0:640] = (gate / (1.0 + jnp.exp(-gate)) * up).astype(BF16)
+        last = tail / (1.0 + jnp.exp(-tail)) * pltpu.roll(tail, 64, 1)
+        hidden[r, 640:768] = jnp.where(lane < 64, last, 0.0).astype(BF16)
+
+
+def forward_kernel(place, normed, mine, ready, other, out, fetched, hidden, partial, sem):
     copy = pltpu.make_async_copy(other, fetched, sem)
     copy.start()
     x = place[0]
-    lane = lax.broadcasted_iota(jnp.int32, (256, 128), 1)
-    for c, weights in enumerate((mine, fetched)):
-        if c == 1:
-            copy.wait()
-
+
+    def products(left, weights, keep):
         @pl.loop(0, 2)
         def _(i):
             r = pl.ds(pl.multiple_of(i * 256, 256), 256)
-            both = jnp.dot(normed[r, :], weights[:, 0:1408], preferred_element_type=F32)
-            gate, up, tail = both[:, 0:640], both[:, 640:1280], both[:, 1280:1408]
-            hidden[r, c * 768 : c * 768 + 640] = (gate / (1.0 + jnp.exp(-gate)) * up).astype(BF16)
-            last = tail / (1.0 + jnp.exp(-tail)) * pltpu.roll(tail, 64, 1)
-            hidden[r, c * 768 + 640 : (c + 1) * 768] = jnp.where(lane < 64, last, 0.0).astype(BF16)
-
-    @pl.loop(0, 2)
-    def _(i):
-        r = pl.ds(pl.multiple_of(i * 256, 256), 256)
-        for j in range(4):
-            start = pl.multiple_of(lax.rem(x + j, 4) * 512, 512)
-            for zz in range(2):
-                n = pl.ds(start + zz * 256, 256)
-                share = dot_nt(hidden[r, 0:768], mine[n, 1408:2176])
-                share += dot_nt(hidden[r, 768:1536], fetched[n, 1408:2176])
-                out[j, r, zz * 256 : (zz + 1) * 256] = share.astype(BF16)
+            for j in range(4):
+                start = pl.multiple_of(lax.rem(x + j, 4) * 512, 512)
+                for zz in range(2):
+                    share = dot_nt(left[r, :], weights[pl.ds(start + zz * 256, 256), 1408:2176])
+                    keep(j, r, slice(zz * 256, (zz + 1) * 256), share)
+
+    def first(j, r, cols, share):
+        partial[j, r, cols] = share
+
+    def second(j, r, cols, share):
+        out[j, r, cols] = (partial[j, r, cols] + share).astype(BF16)
+
+    products(ready, mine, first)
+    copy.wait()
+    gate_rows(normed, fetched, hidden)
+    products(hidden, fetched, second)
 
 
 VM = pl.BlockSpec(memory_space=pltpu.VMEM)
@@ -280,7 +291,7 @@
     )(place, t_own, t_left, t_right, t_low, t_high, *near, *near_other, own_taps, mixer_gain.reshape(4, 512))
     merged = scatter_sum(*pieces)
     second_other = shift(second, "tp_1", 1)
-    *gathered, second = around(merged, "tp_0", second)
+    gathered = around(merged, "tp_0")
 
     normed, first, second = pl.pallas_call(
         norm_kernel,
@@ -298,19 +309,28 @@
         place, t_own, t_left, t_right, jnp.concatenate([t_low, t_high], 0), *gathered,
         merge_gain.reshape(4, 512), channel_gain.reshape(4, 512), second,
     )
+    ready = pl.pallas_call(
+        gate_rows,
+        out_shape=jax.ShapeDtypeStruct((512, 768), BF16),
+        in_specs=[VM] * 2,
+        out_specs=VM,
+        compiler_params=pltpu.CompilerParams(vmem_limit_bytes=20 * 2**20),
+        cost_estimate=pl.CostEstimate(flops=3_000_000_000, bytes_accessed=8_000_000, transcendentals=0),
+    )(normed, second)
     ours = pl.pallas_call(
         forward_kernel,
         out_shape=jax.ShapeDtypeStruct((4, 512, 512), BF16),
-        in_specs=[SM] + [VM] * 2 + [HB],
+        in_specs=[SM] + [VM] * 3 + [HB],
         out_specs=VM,
         scratch_shapes=[
             pltpu.VMEM((2048, 2176), BF16),
-            pltpu.VMEM((512, 1536), BF16),
+            pltpu.VMEM((512, 768), BF16),
+            pltpu.VMEM((4, 512, 512), F32),
             pltpu.SemaphoreType.DMA,
         ],
         compiler_params=pltpu.CompilerParams(vmem_limit_bytes=34 * 2**20),
-        cost_estimate=pl.CostEstimate(flops=9_000_000_000, bytes_accessed=13_000_000, transcendentals=0),
-    )(place, normed, second, second_other)
+        cost_estimate=pl.CostEstimate(flops=6_000_000_000, bytes_accessed=13_000_000, transcendentals=0),
+    )(place, normed, second, ready, second_other)
     pieces = (
         ours[0],
         jnp.concatenate([ours[2, :256], ours[1, 256:]], 0),

time: 285 us -> 286 us (level)
    pallas_call x0 -> x1, Pallas kernels: none -> 3.78 us  [shards(): pl.pallas_call(gate_rows, out_shape=jax.ShapeDtypeStruct((512, 768), BF16...]
  transfers between devices with their start and end apart: 33 -> 33, of which waited for: 19 -> 19; matrix products, arithmetic and copies ran while one was open for 3% -> 3% of each run, Pallas kernels for 4% -> 5%
where the time goes in v3:
time: 286 us
  waiting for transfers between devices  179 us (63%)
  starting transfers between devices  53.9 us (19%)
  Pallas kernels  26.1 us (9%)
  between operations  13.7 us (5%)
  local copies, waits for them, and re-layouts  7.6 us (3%)
  other arithmetic  4.9 us (2%)
    all_gather x1, waiting for transfers between devices, shards(): second = lax.all_gather(second_weights, FS, axis=0, tiled=True)  105 us
    ppermute x31, waiting for transfers between devices, shift(): return lax.ppermute(value, axis, [(i, (i + by) % n) for i in range(n)])  67.5 us
    ppermute x31, starting transfers between devices, shift(): return lax.ppermute(value, axis, [(i, (i + by) % n) for i in range(n)])  49.9 us
    pallas_call x1, Pallas kernels, shards(): pl.pallas_call(forward_kernel, out_shape=jax.ShapeDtypeStruct((4, 512, 51...  9.88 us
    all_to_all x1, waiting for transfers between devices, copy_for_each(): lax.all_to_all(jnp.broadcast_to(value[None], (n, *value.shape)), axis, 0,...  6.68 us
    pallas_call x1, Pallas kernels, shards(): pl.pallas_call(mixer_kernel, out_shape=SHARES, in_specs=[SM] + [VM] * 5 +...  6.08 us
  transfers between devices with their start and end apart: 33, of which 19 were waited for; matrix products, arithmetic and copies ran while one was open for 3% of the time, Pallas kernels for 5%

profile of v3, /device:TPU:1, one launch (start us, length us, event | category | flops | bytes accessed | tf_op | source)
XLA Modules:
  0.0 285.5 jit_solution(7037968214305479212)
XLA Ops:
  6.5 1.8 shard_map.128
  8.3 105.2 %all-gather.2.cloned.1.call-done.arrived = bf16[2048,2176]{1,0:T(8,128)(2,1)} async-done(((bf16[64,2176]{1,0:T(8,128)(2,1)}), bf16[2048,2176]{1,0:T(8,128)(2,1)}) %all-gather.2.cloned.1.call-update) | async-done | bytes 8912912 | tf_op jit(solution)/shard_map/all_gather | solution.py:263
  113.5 1.4 collective-permute-start.22
  114.9 0.8 pad_maximum_fusion.5
  115.7 0.8 broadcast_in_dim.2
  116.5 4.1 %all-to-all-start = ((bf16[8,64,512]{2,1,0:T(8,128)(2,1)}), bf16[8,64,512]{2,1,0:T(8,128)(2,1)S(1)}, u32[]{:S(2)}, u32[]{:S(2)}) async-start(bf16[8,64,512]{2,1,0:T(8,128)(2,1)} %broadcast_in_dim.2), calls=%async_computation | async-start | bytes 1048576 | tf_op jit(solution)/shard_map/all_to_all | solution.py:35
  121.0 8.0 %collective-permute-done = bf16[544,256]{1,0:T(8,128)(2,1)S(1)} collective-permute-done((bf16[544,256]{1,0:T(8,128)(2,1)S(1)}, bf16[544,256]{1,0:T(8,128)(2,1)S(1)}, u32[]{:S(2)}, u32[]{:S(2)}) %collective-permute-start) | collective-permute-done | bytes 278560 | tf_op jit(solution)/shard_map/ppermute | solution.py:19
  129.2 1.3 collective-permute-start.1
  130.5 1.5 collective-permute-start.2
  131.9 6.7 %all-to-all-done.rest_0_ = bf16[8,64,512]{2,1,0:T(8,128)(2,1)S(1)} async-done(((bf16[8,64,512]{2,1,0:T(8,128)(2,1)}), bf16[8,64,512]{2,1,0:T(8,128)(2,1)S(1)}, u32[]{:S(2)}, u32[]{:S(2)}) %all-to-all-start) | async-done | bytes 524320 | tf_op jit(solution)/shard_map/all_to_all | solution.py:35
  138.6 2.7 collective-permute-start.6
  141.3 3.0 %collective-permute-done.1.left.t_left = bf16[544,512]{1,0:T(8,128)(2,1)S(1)} collective-permute-done((bf16[544,512]{1,0:T(8,128)(2,1)S(1)}, bf16[544,512]{1,0:T(8,128)(2,1)S(1)}, u32[]{:S(2)}, u32[]{:S(2)}) %collective-permute-start.1) | collective-permute-done | bytes 557088 | tf_op jit(solution)/shard_map/ppermute | solution.py:19
  144.3 1.2 collective-permute-start.9
  145.7 7.2 %collective-permute-done.5.rest_1_ = bf16[8,64,512]{2,1,0:T(8,128)(2,1)S(1)} collective-permute-done((bf16[8,64,512]{2,1,0:T(8,128)(2,1)S(1)}, bf16[8,64,512]{2,1,0:T(8,128)(2,1)S(1)}, u32[]{:S(2)}, u32[]{:S(2)}) %collective-permute-start.5) | collective-permute-done | bytes 524320 | tf_op jit(solution)/shard_map/ppermute | solution.py:19
  152.9 2.4 collective-permute-start.4
  155.4 1.0 slice.104
  156.4 3.2 %collective-permute-done.4.high = bf16[256,512]{1,0:T(8,128)(2,1)S(1)} collective-permute-done((bf16[256,512]{1,0:T(8,128)(2,1)S(1)}, bf16[256,512]{1,0:T(8,128)(2,1)S(1)}, u32[]{:S(2)}, u32[]{:S(2)}) %collective-permute-start.4) | collective-permute-done | bytes 262176 | tf_op jit(solution)/shard_map/ppermute | solution.py:19
  159.6 2.3 collective-permute-start.10
  161.9 0.8 copy-done.5
  162.8 2.5 collective-permute-start.12
  165.4 3.0 %collective-permute-start.13 = (bf16[4,64,512]{2,1,0:T(8,128)(2,1)}, bf16[4,64,512]{2,1,0:T(8,128)(2,1)}, u32[]{:S(2)}, u32[]{:S(2)}) collective-permute-start(bf16[4,64,512]{2,1,0:T(8,128)(2,1)} %collective-permute-done.8.rest_4_), channel_id=1, source_target_pairs={{0,1},{1,0},{2,3},{3,2},{4,5},{5,4},{6,7},{7,6},{8,9},{9,8},{10,11... | collective-permute-start | bytes 786440 | tf_op jit(solution)/shard_map/ppermute | solution.py:19
  170.0 1.0 copy-done.6
  171.0 6.1 %shard_map.127 = (bf16[512,512]{1,0:T(8,128)(2,1)S(1)}, bf16[512,512]{1,0:T(8,128)(2,1)S(1)}, bf16[512,512]{1,0:T(8,128)(2,1)S(1)}, bf16[256,512]{1,0:T(8,128)(2,1)S(1)}, bf16[256,512]{1,0:T(8,128)(2,1)S(1)}) custom-call(s32[3]{0:T(128)S(1)} %pad_add_fusion.place, bf16[544,512]{1,0:T(8,128)(2,1)S(1)} %maximum_select_fusion.own.t_own, ...), custom_call_target="tpu_custom_call" | custom-call | flops 2300000000 | bytes 9000000 | tf_op jit(solution)/shard_map/pallas_call | solution.py:276
  177.1 3.5 %collective-permute-start.16 = (bf16[512,512]{1,0:T(8,128)(2,1)S(1)}, bf16[512,512]{1,0:T(8,128)(2,1)S(1)}, u32[]{:S(2)}, u32[]{:S(2)}) collective-permute-start(bf16[512,512]{1,0:T(8,128)(2,1)S(1)} %get-tuple-element.25), channel_id=1, source_target_pairs={{0,6},{2,0},{4,2},{6,4},{1,7},{3,1},{5,3},{7,5},{8,14},{10,8},{12,... | collective-permute-start | bytes 1572872 | tf_op jit(solution)/shard_map/ppermute | solution.py:19
  180.6 10.9 %collective-permute-done.16 = bf16[512,512]{1,0:T(8,128)(2,1)S(1)} collective-permute-done((bf16[512,512]{1,0:T(8,128)(2,1)S(1)}, bf16[512,512]{1,0:T(8,128)(2,1)S(1)}, u32[]{:S(2)}, u32[]{:S(2)}) %collective-permute-start.16) | collective-permute-done | bytes 524320 | tf_op jit(solution)/shard_map/ppermute | solution.py:19
  191.6 3.5 %collective-permute-start.17 = (bf16[256,512]{1,0:T(8,128)(2,1)S(1)}, bf16[256,512]{1,0:T(8,128)(2,1)S(1)}, u32[]{:S(2)}, u32[]{:S(2)}) collective-permute-start(bf16[256,512]{1,0:T(8,128)(2,1)S(1)} %add_convert_fusion.2), channel_id=1, source_target_pairs={{0,6},{2,0},{4,2},{6,4},{1,7},{3,1},{5,3},{7,5},{8,14},{10,8},{12,... | collective-permute-start | bytes 786440 | tf_op jit(solution)/shard_map/ppermute | solution.py:19
  195.2 4.3 %collective-permute-done.17 = bf16[256,512]{1,0:T(8,128)(2,1)S(1)} collective-permute-done((bf16[256,512]{1,0:T(8,128)(2,1)S(1)}, bf16[256,512]{1,0:T(8,128)(2,1)S(1)}, u32[]{:S(2)}, u32[]{:S(2)}) %collective-permute-start.17) | collective-permute-done | bytes 262176 | tf_op jit(solution)/shard_map/ppermute | solution.py:19
  199.5 3.3 %collective-permute-done.15 = bf16[256,512]{1,0:T(8,128)(2,1)S(1)} collective-permute-done((bf16[256,512]{1,0:T(8,128)(2,1)S(1)}, bf16[256,512]{1,0:T(8,128)(2,1)S(1)}, u32[]{:S(2)}, u32[]{:S(2)}) %collective-permute-start.15) | collective-permute-done | bytes 262176 | tf_op jit(solution)/shard_map/ppermute | solution.py:19
  203.2 2.7 collective-permute-start.19
  205.8 9.7 %collective-permute-done.18.m_left = bf16[512,512]{1,0:T(8,128)(2,1)S(1)} collective-permute-done((bf16[512,512]{1,0:T(8,128)(2,1)S(1)}, bf16[512,512]{1,0:T(8,128)(2,1)S(1)}, u32[]{:S(2)}, u32[]{:S(2)}) %collective-permute-start.18) | collective-permute-done | bytes 524320 | tf_op jit(solution)/shard_map/ppermute | solution.py:19
  216.9 2.7 collective-permute-start.21
  220.3 1.0 pad_maximum_fusion.t_far
  221.3 1.6 collective-permute-done.20.m_low
  223.2 4.6 %shard_map.129 = (bf16[512,2048]{1,0:T(8,128)(2,1)S(1)}, bf16[512,512]{1,0:T(8,128)(2,1)S(1)}, bf16[2048,2176]{1,0:T(8,128)(2,1)S(1)}) custom-call(s32[3]{0:T(128)S(1)} %copy-done.4, bf16[544,512]{1,0:T(8,128)(2,1)S(1)} %maximum_select_fusion.own.t_own, bf16[544,512]{1,0:T(8,128)(2,1)S(1)} %collective-permute-done.1.left.t_left, ...), custom_call_target="tpu_custom_call" | custom-call | flops 30000000 | bytes 6500000 | tf_op jit(solution)/shard_map/pallas_call | solution.py:296
  227.8 0.8 copy-done
  228.6 3.8 %shard_map.130.ready = bf16[512,768]{1,0:T(8,128)(2,1)S(1)} custom-call(bf16[512,2048]{1,0:T(8,128)(2,1)S(1)} %get-tuple-element.31.normed, bf16[2048,2176]{1,0:T(8,128)(2,1)S(1)} %get-tuple-element.32.weights.mine), custom_call_target="tpu_custom_call" | custom-call | flops 3000000000 | bytes 8000000 | tf_op jit(solution)/shard_map/pallas_call | solution.py:312
  232.4 9.9 %shard_map.131 = bf16[4,512,512]{2,1,0:T(8,128)(2,1)S(1)} custom-call(s32[3]{0:T(128)S(1)} %copy-done.4, bf16[512,2048]{1,0:T(8,128)(2,1)S(1)} %get-tuple-element.31.normed, bf16[2048,2176]{1,0:T(8,128)(2,1)S(1)} %get-tuple-element.32.weights.mine, bf16[512,768]{1,0:T(8,128)(2,1)S(1)} %shard_map.130.ready, bf16[2048,2176]{1,0:T(8,128)(2,1)} %collective-permute-done.22.other), custom_call_target="tpu_custom_call" | custom-call | flops 6000000000 | bytes 13000000 | tf_op jit(solution)/shard_map/pallas_call | solution.py:320
  242.5 3.2 %collective-permute-start.25 = (bf16[512,512]{1,0:T(8,128)(2,1)S(1)}, bf16[512,512]{1,0:T(8,128)(2,1)S(1)}, u32[]{:S(2)}, u32[]{:S(2)}) collective-permute-start(bf16[512,512]{1,0:T(8,128)(2,1)S(1)} %pad_maximum_fusion.3), channel_id=1, source_target_pairs={{0,6},{2,0},{4,2},{6,4},{1,7},{3,1},{5,3},{7,5},{8,14},{10,8},{12,... | collective-permute-start | bytes 1572872 | tf_op jit(solution)/shard_map/ppermute | solution.py:19
  245.7 7.5 %collective-permute-done.23 = bf16[512,512]{1,0:T(8,128)(2,1)S(1)} collective-permute-done((bf16[512,512]{1,0:T(8,128)(2,1)S(1)}, bf16[512,512]{1,0:T(8,128)(2,1)S(1)}, u32[]{:S(2)}, u32[]{:S(2)}) %collective-permute-start.23) | collective-permute-done | bytes 524320 | tf_op jit(solution)/shard_map/ppermute | solution.py:19
  254.2 2.0 collective-permute-start.26
  256.2 4.4 %collective-permute-done.24 = bf16[256,512]{1,0:T(8,128)(2,1)S(1)} collective-permute-done((bf16[256,512]{1,0:T(8,128)(2,1)S(1)}, bf16[256,512]{1,0:T(8,128)(2,1)S(1)}, u32[]{:S(2)}, u32[]{:S(2)}) %collective-permute-start.24) | collective-permute-done | bytes 262176 | tf_op jit(solution)/shard_map/ppermute | solution.py:19
  261.0 1.0 collective-permute-start.27
  262.0 1.9 collective-permute-start.28
  264.0 1.3 collective-permute-start.29
  266.1 1.8 collective-permute-done.29
  268.2 8.3 %collective-permute-start.30 = (bf16[512,256]{1,0:T(8,128)(2,1)S(1)}, bf16[512,256]{1,0:T(8,128)(2,1)S(1)}, u32[]{:S(2)}, u32[]{:S(2)}) collective-permute-start(bf16[512,256]{1,0:T(8,128)(2,1)S(1)} %get-tuple-element.46), channel_id=1, source_target_pairs={{0,1},{1,0},{2,3},{3,2},{4,5},{5,4},{6,7},{7,6},{8,9},{9,8},{10,11... | collective-permute-start | bytes 786440 | tf_op jit(solution)/shard_map/ppermute | solution.py:19
  276.5 1.2 collective-permute-done.30
  277.7 1.0 maximum_select_fusion.1
  (75 shorter events, 8.2 us)
Async XLA Ops:
  6.5 107.0 %all-gather.2.cloned.1.call-start = ((), (), s32[]{:S(2)}) async-start(), calls=%async_computation.1 | async-start | bytes 9191424 | tf_op jit(solution)/shard_map/all_gather | solution.py:263
  8.3 112.3 %copy-start.7 = (bf16[1024,256]{1,0:T(8,128)(2,1)S(1)}, bf16[1024,256]{1,0:T(8,128)(2,1)}, u32[]{:S(2)}) copy-start(bf16[1024,256]{1,0:T(8,128)(2,1)} %param.13) | copy-start | bytes 1572868
  113.5 118.9 %collective-permute-start.22 = (bf16[2048,2176]{1,0:T(8,128)(2,1)}, bf16[2048,2176]{1,0:T(8,128)(2,1)}, u32[]{:S(2)}, u32[]{:S(2)}) collective-permute-start(bf16[2048,2176]{1,0:T(8,128)(2,1)} %all-gather.2.cloned.1.call-done.arrived), channel_id=1, source_target_pairs={{0,1},{1,0},{2,3},{3,2},{4,5},{5,4},{6,7},{7,6},{8,9},{9,8},{10,11... | collective-permute-start | bytes 26738696 | tf_op jit(solution)/shard_map/ppermute | solution.py:19
  116.5 22.1 %all-to-all-start = ((bf16[8,64,512]{2,1,0:T(8,128)(2,1)}), bf16[8,64,512]{2,1,0:T(8,128)(2,1)S(1)}, u32[]{:S(2)}, u32[]{:S(2)}) async-start(bf16[8,64,512]{2,1,0:T(8,128)(2,1)} %broadcast_in_dim.2), calls=%async_computation | async-start | bytes 1048576 | tf_op jit(solution)/shard_map/all_to_all | solution.py:35
  120.7 8.4 %collective-permute-start = (bf16[544,256]{1,0:T(8,128)(2,1)S(1)}, bf16[544,256]{1,0:T(8,128)(2,1)S(1)}, u32[]{:S(2)}, u32[]{:S(2)}) collective-permute-start(bf16[544,256]{1,0:T(8,128)(2,1)S(1)} %get-tuple-element.50), channel_id=1, source_target_pairs={{0,1},{1,0},{2,3},{3,2},{4,5},{5,4},{6,7},{7,6},{8,9},{9,8},{10,11... | collective-permute-start | bytes 835592 | tf_op jit(solution)/shard_map/ppermute | solution.py:19
  129.2 39.3 %copy-start.8 = (f32[2048]{0:T(1024)S(1)}, f32[2048]{0:T(1024)}, u32[]{:S(2)}) copy-start(f32[2048]{0:T(1024)} %param.14) | copy-start | bytes 24580
  129.2 15.1 %collective-permute-start.1 = (bf16[544,512]{1,0:T(8,128)(2,1)S(1)}, bf16[544,512]{1,0:T(8,128)(2,1)S(1)}, u32[]{:S(2)}, u32[]{:S(2)}) collective-permute-start(bf16[544,512]{1,0:T(8,128)(2,1)S(1)} %maximum_select_fusion.own.t_own), channel_id=1, source_target_pairs={{0,2},{2,4},{4,6},{6,0},{1,3},{3,5},{5,7},{7,1},{8,10},{10,12},{12... | collective-permute-start | bytes 1671176 | tf_op jit(solution)/shard_map/ppermute | solution.py:19
  130.5 15.1 %collective-permute-start.2 = (bf16[544,512]{1,0:T(8,128)(2,1)S(1)}, bf16[544,512]{1,0:T(8,128)(2,1)S(1)}, u32[]{:S(2)}, u32[]{:S(2)}) collective-permute-start(bf16[544,512]{1,0:T(8,128)(2,1)S(1)} %maximum_select_fusion.own.t_own), channel_id=1, source_target_pairs={{0,6},{2,0},{4,2},{6,4},{1,7},{3,1},{5,3},{7,5},{8,14},{10,8},{12,... | collective-permute-start | bytes 1671176 | tf_op jit(solution)/shard_map/ppermute | solution.py:19
  138.6 14.2 %collective-permute-start.5 = (bf16[8,64,512]{2,1,0:T(8,128)(2,1)S(1)}, bf16[8,64,512]{2,1,0:T(8,128)(2,1)S(1)}, u32[]{:S(2)}, u32[]{:S(2)}) collective-permute-start(bf16[8,64,512]{2,1,0:T(8,128)(2,1)S(1)} %all-to-all-done.rest_0_), channel_id=1, source_target_pairs={{0,8},{8,16},{16,24},{24,0},{1,9},{9,17},{17,25},{25,1},{2,10},{10... | collective-permute-start | bytes 1572872 | tf_op jit(solution)/shard_map/ppermute | solution.py:19
  138.6 16.7 %collective-permute-start.6 = (bf16[8,64,512]{2,1,0:T(8,128)(2,1)S(1)}, bf16[8,64,512]{2,1,0:T(8,128)(2,1)}, u32[]{:S(2)}, u32[]{:S(2)}) collective-permute-start(bf16[8,64,512]{2,1,0:T(8,128)(2,1)S(1)} %all-to-all-done.rest_0_), channel_id=1, source_target_pairs={{0,24},{8,0},{16,8},{24,16},{1,25},{9,1},{17,9},{25,17},{2,26},{10... | collective-permute-start | bytes 1572872 | tf_op jit(solution)/shard_map/ppermute | solution.py:19
  144.3 17.6 %collective-permute-start.9 = (bf16[8,64,512]{2,1,0:T(8,128)(2,1)S(1)}, bf16[8,64,512]{2,1,0:T(8,128)(2,1)S(1)}, u32[]{:S(2)}, u32[]{:S(2)}) collective-permute-start(bf16[8,64,512]{2,1,0:T(8,128)(2,1)S(1)} %all-to-all-done.rest_0_), channel_id=1, source_target_pairs={{0,1},{1,0},{2,3},{3,2},{4,5},{5,4},{6,7},{7,6},{8,9},{9,8},{10,11... | collective-permute-start | bytes 1572872 | tf_op jit(solution)/shard_map/ppermute | solution.py:19
  145.6 14.1 %collective-permute-start.3 = (bf16[288,512]{1,0:T(8,128)(2,1)S(1)}, bf16[288,512]{1,0:T(8,128)(2,1)S(1)}, u32[]{:S(2)}, u32[]{:S(2)}) collective-permute-start(bf16[288,512]{1,0:T(8,128)(2,1)S(1)} %slice.101), channel_id=1, source_target_pairs={{0,2},{2,4},{4,6},{6,0},{1,3},{3,5},{5,7},{7,1},{8,10},{10,12},{12... | collective-permute-start | bytes 884744 | tf_op jit(solution)/shard_map/ppermute | solution.py:19
  152.9 6.8 %collective-permute-start.4 = (bf16[256,512]{1,0:T(8,128)(2,1)S(1)}, bf16[256,512]{1,0:T(8,128)(2,1)S(1)}, u32[]{:S(2)}, u32[]{:S(2)}) collective-permute-start(bf16[256,512]{1,0:T(8,128)(2,1)S(1)} %slice.102), channel_id=1, source_target_pairs={{0,6},{2,0},{4,2},{6,4},{1,7},{3,1},{5,3},{7,5},{8,14},{10,8},{12,... | collective-permute-start | bytes 786440 | tf_op jit(solution)/shard_map/ppermute | solution.py:19
  155.3 7.6 %collective-permute-start.7 = (bf16[4,64,512]{2,1,0:T(8,128)(2,1)S(1)}, bf16[4,64,512]{2,1,0:T(8,128)(2,1)S(1)}, u32[]{:S(2)}, u32[]{:S(2)}) collective-permute-start(bf16[4,64,512]{2,1,0:T(8,128)(2,1)S(1)} %slice.103), channel_id=1, source_target_pairs={{0,8},{8,16},{16,24},{24,0},{1,9},{9,17},{17,25},{25,1},{2,10},{10... | collective-permute-start | bytes 786440 | tf_op jit(solution)/shard_map/ppermute | solution.py:19
  159.6 17.5 %copy-start.2 = (bf16[256,512]{1,0:T(8,128)(2,1)}, bf16[256,512]{1,0:T(8,128)(2,1)S(1)}, u32[]{:S(2)}) copy-start(bf16[256,512]{1,0:T(8,128)(2,1)S(1)} %collective-permute-done.4.high) | copy-start | bytes 786436
  159.6 5.8 %collective-permute-start.8 = (bf16[4,64,512]{2,1,0:T(8,128)(2,1)S(1)}, bf16[4,64,512]{2,1,0:T(8,128)(2,1)}, u32[]{:S(2)}, u32[]{:S(2)}) collective-permute-start(bf16[4,64,512]{2,1,0:T(8,128)(2,1)S(1)} %slice.104), channel_id=1, source_target_pairs={{0,24},{8,0},{16,8},{24,16},{1,25},{9,1},{17,9},{25,17},{2,26},{10... | collective-permute-start | bytes 786440 | tf_op jit(solution)/shard_map/ppermute | solution.py:19
  159.6 10.3 %collective-permute-start.10 = (bf16[8,64,512]{2,1,0:T(8,128)(2,1)S(1)}, bf16[8,64,512]{2,1,0:T(8,128)(2,1)}, u32[]{:S(2)}, u32[]{:S(2)}) collective-permute-start(bf16[8,64,512]{2,1,0:T(8,128)(2,1)S(1)} %collective-permute-done.5.rest_1_), channel_id=1, source_target_pairs={{0,1},{1,0},{2,3},{3,2},{4,5},{5,4},{6,7},{7,6},{8,9},{9,8},{10,11... | collective-permute-start | bytes 1572872 | tf_op jit(solution)/shard_map/ppermute | solution.py:19
  161.9 0.8 copy-start.5
  162.7 7.3 %collective-permute-start.11 = (bf16[8,64,512]{2,1,0:T(8,128)(2,1)}, bf16[8,64,512]{2,1,0:T(8,128)(2,1)}, u32[]{:S(2)}, u32[]{:S(2)}) collective-permute-start(bf16[8,64,512]{2,1,0:T(8,128)(2,1)} %collective-permute-done.6.rest_2_), channel_id=1, source_target_pairs={{0,1},{1,0},{2,3},{3,2},{4,5},{5,4},{6,7},{7,6},{8,9},{9,8},{10,11... | collective-permute-start | bytes 1572872 | tf_op jit(solution)/shard_map/ppermute | solution.py:19
  162.8 6.4 %collective-permute-start.12 = (bf16[4,64,512]{2,1,0:T(8,128)(2,1)S(1)}, bf16[4,64,512]{2,1,0:T(8,128)(2,1)}, u32[]{:S(2)}, u32[]{:S(2)}) collective-permute-start(bf16[4,64,512]{2,1,0:T(8,128)(2,1)S(1)} %collective-permute-done.7.rest_3_), channel_id=1, source_target_pairs={{0,1},{1,0},{2,3},{3,2},{4,5},{5,4},{6,7},{7,6},{8,9},{9,8},{10,11... | collective-permute-start | bytes 786440 | tf_op jit(solution)/shard_map/ppermute | solution.py:19
  165.4 4.5 %collective-permute-start.13 = (bf16[4,64,512]{2,1,0:T(8,128)(2,1)}, bf16[4,64,512]{2,1,0:T(8,128)(2,1)}, u32[]{:S(2)}, u32[]{:S(2)}) collective-permute-start(bf16[4,64,512]{2,1,0:T(8,128)(2,1)} %collective-permute-done.8.rest_4_), channel_id=1, source_target_pairs={{0,1},{1,0},{2,3},{3,2},{4,5},{5,4},{6,7},{7,6},{8,9},{9,8},{10,11... | collective-permute-start | bytes 786440 | tf_op jit(solution)/shard_map/ppermute | solution.py:19
  168.5 8.6 %copy-start.3 = (s32[3]{0:T(128)}, s32[3]{0:T(128)S(1)}, u32[]{:S(2)}) copy-start(s32[3]{0:T(128)S(1)} %pad_add_fusion.place) | copy-start | bytes 40
  169.9 1.0 copy-start.6
  177.1 14.4 %collective-permute-start.16 = (bf16[512,512]{1,0:T(8,128)(2,1)S(1)}, bf16[512,512]{1,0:T(8,128)(2,1)S(1)}, u32[]{:S(2)}, u32[]{:S(2)}) collective-permute-start(bf16[512,512]{1,0:T(8,128)(2,1)S(1)} %get-tuple-element.25), channel_id=1, source_target_pairs={{0,6},{2,0},{4,2},{6,4},{1,7},{3,1},{5,3},{7,5},{8,14},{10,8},{12,... | collective-permute-start | bytes 1572872 | tf_op jit(solution)/shard_map/ppermute | solution.py:19
  180.6 14.5 %collective-permute-start.14 = (bf16[512,512]{1,0:T(8,128)(2,1)S(1)}, bf16[512,512]{1,0:T(8,128)(2,1)S(1)}, u32[]{:S(2)}, u32[]{:S(2)}) collective-permute-start(bf16[512,512]{1,0:T(8,128)(2,1)S(1)} %get-tuple-element.23), channel_id=1, source_target_pairs={{0,2},{2,4},{4,6},{6,0},{1,3},{3,5},{5,7},{7,1},{8,10},{10,12},{12... | collective-permute-start | bytes 1572872 | tf_op jit(solution)/shard_map/ppermute | solution.py:19
  191.6 7.9 %collective-permute-start.17 = (bf16[256,512]{1,0:T(8,128)(2,1)S(1)}, bf16[256,512]{1,0:T(8,128)(2,1)S(1)}, u32[]{:S(2)}, u32[]{:S(2)}) collective-permute-start(bf16[256,512]{1,0:T(8,128)(2,1)S(1)} %add_convert_fusion.2), channel_id=1, source_target_pairs={{0,6},{2,0},{4,2},{6,4},{1,7},{3,1},{5,3},{7,5},{8,14},{10,8},{12,... | collective-permute-start | bytes 786440 | tf_op jit(solution)/shard_map/ppermute | solution.py:19
  195.1 7.7 %collective-permute-start.15 = (bf16[256,512]{1,0:T(8,128)(2,1)S(1)}, bf16[256,512]{1,0:T(8,128)(2,1)S(1)}, u32[]{:S(2)}, u32[]{:S(2)}) collective-permute-start(bf16[256,512]{1,0:T(8,128)(2,1)S(1)} %add_convert_fusion.3), channel_id=1, source_target_pairs={{0,2},{2,4},{4,6},{6,0},{1,3},{3,5},{5,7},{7,1},{8,10},{10,12},{12... | collective-permute-start | bytes 786440 | tf_op jit(solution)/shard_map/ppermute | solution.py:19
  203.0 16.6 %copy-start.9 = (f32[2048]{0:T(1024)S(1)}, f32[2048]{0:T(1024)}, u32[]{:S(2)}) copy-start(f32[2048]{0:T(1024)} %param.20) | copy-start | bytes 24580
  203.1 12.4 %collective-permute-start.18 = (bf16[512,512]{1,0:T(8,128)(2,1)S(1)}, bf16[512,512]{1,0:T(8,128)(2,1)S(1)}, u32[]{:S(2)}, u32[]{:S(2)}) collective-permute-start(bf16[512,512]{1,0:T(8,128)(2,1)S(1)} %pad_maximum_fusion.1.m_own), channel_id=1, source_target_pairs={{0,2},{2,4},{4,6},{6,0},{1,3},{3,5},{5,7},{7,1},{8,10},{10,12},{12... | collective-permute-start | bytes 1572872 | tf_op jit(solution)/shard_map/ppermute | solution.py:19
  203.2 13.0 %collective-permute-start.19 = (bf16[512,512]{1,0:T(8,128)(2,1)S(1)}, bf16[512,512]{1,0:T(8,128)(2,1)S(1)}, u32[]{:S(2)}, u32[]{:S(2)}) collective-permute-start(bf16[512,512]{1,0:T(8,128)(2,1)S(1)} %pad_maximum_fusion.1.m_own), channel_id=1, source_target_pairs={{0,6},{2,0},{4,2},{6,4},{1,7},{3,1},{5,3},{7,5},{8,14},{10,8},{12,... | collective-permute-start | bytes 1572872 | tf_op jit(solution)/shard_map/ppermute | solution.py:19
  216.2 6.7 %collective-permute-start.20 = (bf16[256,512]{1,0:T(8,128)(2,1)}, bf16[256,512]{1,0:T(8,128)(2,1)}, u32[]{:S(2)}, u32[]{:S(2)}) collective-permute-start(bf16[256,512]{1,0:T(8,128)(2,1)} %slice.107), channel_id=1, source_target_pairs={{0,2},{2,4},{4,6},{6,0},{1,3},{3,5},{5,7},{7,1},{8,10},{10,12},{12... | collective-permute-start | bytes 786440 | tf_op jit(solution)/shard_map/ppermute | solution.py:19
  216.9 6.3 %collective-permute-start.21 = (bf16[256,512]{1,0:T(8,128)(2,1)}, bf16[256,512]{1,0:T(8,128)(2,1)}, u32[]{:S(2)}, u32[]{:S(2)}) collective-permute-start(bf16[256,512]{1,0:T(8,128)(2,1)} %slice.108), channel_id=1, source_target_pairs={{0,6},{2,0},{4,2},{6,4},{1,7},{3,1},{5,3},{7,5},{8,14},{10,8},{12,... | collective-permute-start | bytes 786440 | tf_op jit(solution)/shard_map/ppermute | solution.py:19
  220.3 2.9 %copy-start.4 = (s32[3]{0:T(128)S(1)}, s32[3]{0:T(128)}, u32[]{:S(2)}) copy-start(s32[3]{0:T(128)} %copy-done.3) | copy-start | bytes 40
  227.8 0.8 copy-start
  242.4 10.8 %collective-permute-start.23 = (bf16[512,512]{1,0:T(8,128)(2,1)S(1)}, bf16[512,512]{1,0:T(8,128)(2,1)S(1)}, u32[]{:S(2)}, u32[]{:S(2)}) collective-permute-start(bf16[512,512]{1,0:T(8,128)(2,1)S(1)} %pad_maximum_fusion.2), channel_id=1, source_target_pairs={{0,2},{2,4},{4,6},{6,0},{1,3},{3,5},{5,7},{7,1},{8,10},{10,12},{12... | collective-permute-start | bytes 1572872 | tf_op jit(solution)/shard_map/ppermute | solution.py:19
  242.5 10.7 %collective-permute-start.25 = (bf16[512,512]{1,0:T(8,128)(2,1)S(1)}, bf16[512,512]{1,0:T(8,128)(2,1)S(1)}, u32[]{:S(2)}, u32[]{:S(2)}) collective-permute-start(bf16[512,512]{1,0:T(8,128)(2,1)S(1)} %pad_maximum_fusion.3), channel_id=1, source_target_pairs={{0,6},{2,0},{4,2},{6,4},{1,7},{3,1},{5,3},{7,5},{8,14},{10,8},{12,... | collective-permute-start | bytes 1572872 | tf_op jit(solution)/shard_map/ppermute | solution.py:19
  253.4 7.2 %collective-permute-start.24 = (bf16[256,512]{1,0:T(8,128)(2,1)S(1)}, bf16[256,512]{1,0:T(8,128)(2,1)S(1)}, u32[]{:S(2)}, u32[]{:S(2)}) collective-permute-start(bf16[256,512]{1,0:T(8,128)(2,1)S(1)} %get-tuple-element.40), channel_id=1, source_target_pairs={{0,2},{2,4},{4,6},{6,0},{1,3},{3,5},{5,7},{7,1},{8,10},{10,12},{12... | collective-permute-start | bytes 786440 | tf_op jit(solution)/shard_map/ppermute | solution.py:19
  254.2 13.7 %copy-start.1 = (bf16[512,512]{1,0:T(8,128)(2,1)S(1)}, bf16[512,512]{1,0:T(8,128)(2,1)}, u32[]{:S(2)}) copy-start(bf16[512,512]{1,0:T(8,128)(2,1)} %copy-done) | copy-start | bytes 1572868
  254.2 6.4 %collective-permute-start.26 = (bf16[256,512]{1,0:T(8,128)(2,1)S(1)}, bf16[256,512]{1,0:T(8,128)(2,1)S(1)}, u32[]{:S(2)}, u32[]{:S(2)}) collective-permute-start(bf16[256,512]{1,0:T(8,128)(2,1)S(1)} %get-tuple-element.39), channel_id=1, source_target_pairs={{0,6},{2,0},{4,2},{6,4},{1,7},{3,1},{5,3},{7,5},{8,14},{10,8},{12,... | collective-permute-start | bytes 786440 | tf_op jit(solution)/shard_map/ppermute | solution.py:19
  261.0 5.1 %collective-permute-start.27 = (f32[4,128]{1,0:T(4,128)S(1)}, f32[4,128]{1,0:T(4,128)S(1)}, u32[]{:S(2)}, u32[]{:S(2)}) collective-permute-start(f32[4,128]{1,0:T(4,128)S(1)} %bitcast.39), channel_id=1, source_target_pairs={{0,2},{2,4},{4,6},{6,0},{1,3},{3,5},{5,7},{7,1},{8,10},{10,12},{12... | collective-permute-start | bytes 6152 | tf_op jit(solution)/shard_map/ppermute | solution.py:19
  262.0 4.0 %collective-permute-start.28 = (f32[4,128]{1,0:T(4,128)S(1)}, f32[4,128]{1,0:T(4,128)S(1)}, u32[]{:S(2)}, u32[]{:S(2)}) collective-permute-start(f32[4,128]{1,0:T(4,128)S(1)} %bitcast.40), channel_id=1, source_target_pairs={{0,6},{2,0},{4,2},{6,4},{1,7},{3,1},{5,3},{7,5},{8,14},{10,8},{12,... | collective-permute-start | bytes 6152 | tf_op jit(solution)/shard_map/ppermute | solution.py:19
  264.0 3.9 %collective-permute-start.29 = (f32[4,128]{1,0:T(4,128)S(1)}, f32[4,128]{1,0:T(4,128)S(1)}, u32[]{:S(2)}, u32[]{:S(2)}) collective-permute-start(f32[4,128]{1,0:T(4,128)S(1)} %bitcast.41), channel_id=1, source_target_pairs={{0,4},{2,6},{4,0},{6,2},{1,5},{3,7},{5,1},{7,3},{8,12},{10,14},{12... | collective-permute-start | bytes 6152 | tf_op jit(solution)/shard_map/ppermute | solution.py:19
  268.2 9.4 %collective-permute-start.30 = (bf16[512,256]{1,0:T(8,128)(2,1)S(1)}, bf16[512,256]{1,0:T(8,128)(2,1)S(1)}, u32[]{:S(2)}, u32[]{:S(2)}) collective-permute-start(bf16[512,256]{1,0:T(8,128)(2,1)S(1)} %get-tuple-element.46), channel_id=1, source_target_pairs={{0,1},{1,0},{2,3},{3,2},{4,5},{5,4},{6,7},{7,6},{8,9},{9,8},{10,11... | collective-permute-start | bytes 786440 | tf_op jit(solution)/shard_map/ppermute | solution.py:19
Sparse Core Ops, SparseCore 0:
  9.9 103.5 all-gather.1
